TPU v7x, 32 devices: a whole 2x2x4 slice. The times are simulated.
32 devices in a mesh: fs: 8 (over z, x), tp: 4 (over y, core).
Axes of the slice: x: 2, y: 2, z: 4, core: 2. Of those that a mesh axis runs over, the one named last changes fastest.
Arguments:
- saved_input: bfloat16 [49152, 2048], P(('fs', 'tp')), may hold values from -6 to 6
- value_cotangent: bfloat16 [49152, 1024], P(('fs', 'tp')), may hold values from -0.0546875 to 0.0546875
- decay_cotangent: bfloat16 [49152, 16], P(('fs', 'tp')), may hold values from -0.02734375 to 0.02734375
- value_master: float32 [2048, 1024], P('fs', 'tp'), may hold values from -6 to 6
- value_factor: bfloat16 [2048, 256], P('fs'), may hold values from -0.22097087 to 0.22097087
- value_mean: float32 [256, 1024], P('fs', 'tp'), may hold values from -0.625 to 0.625
- value_second: float32 [256, 1024], P('fs', 'tp'), may hold values from 0.0001 to 0.1
- decay_master: float32 [2048, 16], replicated, may hold values from -6 to 6
- decay_mean: float32 [2048, 16], replicated, may hold values from -0.625 to 0.625
- decay_second: float32 [2048, 16], replicated, may hold values from 0.001 to 0.01
Outputs:
- value_step: float32 [2048, 1024], P('fs', 'tp')
- value_new: float32 [2048, 1024], P('fs', 'tp')
- value_copy: bfloat16 [2048, 1024], P(None, 'tp')
- mean_new: float32 [256, 1024], P('fs', 'tp')
- second_new: float32 [256, 1024], P('fs', 'tp')
- decay_step: float32 [2048, 16], replicated
- decay_copy: bfloat16 [2048, 16], replicated
All inputs are finite; a program needn't handle non-finite values.
Results may differ from a plain program's by a relative error of at most 0.0004.
Values may be sent and summed in bfloat16 or wider, within the bound.
No kernel may reach another device: no remote copies, remote signals or barrier semaphores. Data moves between devices by JAX's collectives and lax.ppermute only.
A program may use at most 64 MiB of HBM per device.

v0:
```python
import jax
import jax.numpy as jnp
from jax import lax
from jax.sharding import PartitionSpec as P

D = 2048
GW = 1024


BETA_ONE = 0.9
BETA_TWO = 0.99
ADAM_EPS = 1e-08
RMS_EPS = 1e-06
LEARN_RATE = 0.05
TOKEN_DIMS = (((0,), (0,)), ((), ()))


def adam_direction(moment_one, moment_two, gradient):
    mean_new = BETA_ONE * moment_one + (1.0 - BETA_ONE) * gradient
    second_new = BETA_TWO * moment_two + (1.0 - BETA_TWO) * gradient * gradient
    return (mean_new, second_new, mean_new / (jnp.sqrt(second_new) + ADAM_EPS))


def block_sum(left_parts, right_side):
    fs_count = lax.axis_size("fs")
    result = jnp.zeros(
        (lax.axis_size("fs") * (left_parts[0].shape[1] // fs_count), right_side.shape[1]),
        jnp.float32,
    )
    for left_side in left_parts:
        result = result + lax.dot_general(
            left_side, right_side, TOKEN_DIMS, preferred_element_type=jnp.float32
        )
    row_block = lax.psum_scatter(result, "fs", scatter_dimension=0, tiled=True)
    return lax.psum_scatter(row_block, "tp", scatter_dimension=1, tiled=True)


def local(
    saved_input,
    value_cotangent,
    decay_cotangent,
    value_master,
    value_factor,
    value_mean,
    value_second,
    decay_master,
    decay_mean,
    decay_second,
):
    decay_local = lax.dot_general(
        saved_input, decay_cotangent, TOKEN_DIMS, preferred_element_type=jnp.float32
    )
    decay_grad = lax.psum(decay_local, ("fs", "tp"))
    unused_mean, unused_second, decay_step = adam_direction(decay_mean, decay_second, decay_grad)
    decay_copy = (decay_master - LEARN_RATE * decay_step).astype(jnp.bfloat16)
    factor_wide = value_factor.astype(jnp.float32)
    mapped = jnp.dot(
        saved_input,
        lax.all_gather(value_factor, "fs", axis=0, tiled=True),
        preferred_element_type=jnp.float32,
    )
    high_part = lax.optimization_barrier(mapped.astype(jnp.bfloat16))
    low_part = (mapped - high_part.astype(jnp.float32)).astype(jnp.bfloat16)
    projected = block_sum((high_part, low_part), value_cotangent)
    mean_new, second_new, direction = adam_direction(value_mean, value_second, projected)
    raw_update = jnp.dot(
        factor_wide,
        lax.all_gather(direction, "fs", axis=0, tiled=True),
        precision=lax.Precision.HIGHEST,
        preferred_element_type=jnp.float32,
    )
    squares = lax.psum(jnp.sum(raw_update * raw_update), ("fs", "tp"))
    value_step = raw_update * lax.rsqrt(squares / (D * GW) + RMS_EPS)
    value_new = value_master - LEARN_RATE * value_step
    value_copy = lax.all_gather(value_new.astype(jnp.bfloat16), "fs", axis=0, tiled=True)
    return (value_step, value_new, value_copy, mean_new, second_new, decay_step, decay_copy)


def solution(mesh):
    in_specs = (
        P(("fs", "tp"), None),
        P(("fs", "tp"), None),
        P(("fs", "tp"), None),
        P("fs", "tp"),
        P("fs", None),
        P("fs", "tp"),
        P("fs", "tp"),
        P(),
        P(),
        P(),
    )
    out_specs = (
        P("fs", "tp"),
        P("fs", "tp"),
        P(None, "tp"),
        P("fs", "tp"),
        P("fs", "tp"),
        P(),
        P(),
    )
    return jax.shard_map(local, mesh=mesh, in_specs=in_specs, out_specs=out_specs, check_vma=False)
```

profile of v0, /device:TPU:0, one launch (start us, length us, event | category | flops | bytes accessed | tf_op | source)
XLA Modules:
  0.0 273.7 jit_solution(16057867461915626292)
XLA Ops:
  8.0 0.0 copy-start
  8.0 0.0 all-gather.3.cloned.1.call-start
  8.1 0.7 all-gather.3.cloned.1.call-update
  8.7 0.0 reduce-scatter.3.cloned.1.call-start
  8.8 45.2 %all-gather.3.cloned.1.call-done = bf16[2048,256]{1,0:T(8,128)(2,1)} async-done(((bf16[256,256]{1,0:T(8,128)(2,1)}), bf16[2048,256]{1,0:T(8,128)(2,1)}) %all-gather.3.cloned.1.call-update) | async-done | bytes 1048592 | tf_op jit(solution)/shard_map/all_gather | solution.py:59
  54.0 5.0 %fusion.8 = (bf16[1536,256]{1,0:T(8,128)(2,1)S(1)}, f32[1536,256]{1,0:T(8,128)S(1)}) fusion(bf16[1536,2048]{1,0:T(8,128)(2,1)} %param.10, bf16[2048,256]{1,0:T(8,128)(2,1)} %all-gather.3.cloned.1.call-done), kind=kOutput, calls=%fused_computation.16 | convolution fusion | flops 1611005952 | bytes 9699328 | tf_op jit(solution)/shard_map/dot_general | solution.py:57
  59.0 0.0 copy-done
  59.0 1.0 fusion.9
  60.0 0.0 copy-start.2
  60.0 2.0 convolution_add_fusion
  62.1 0.0 reduce-scatter.3.cloned.1.call-update
  62.1 0.0 reduce-scatter.5.cloned.1.call-start
  62.1 63.1 %reduce-scatter.3.cloned.1.call-done = f32[32,1024]{1,0:T(8,128)} async-done(((f32[256,1024]{1,0:T(8,128)}), f32[32,1024]{1,0:T(8,128)}) %reduce-scatter.3.cloned.1.call-update) | async-done | bytes 131088 | tf_op jit(solution)/shard_map/reduce_scatter | solution.py:34
  125.2 0.0 reduce-scatter.5.cloned.1.call-update
  125.2 0.0 copy-start.1
  125.2 0.0 all-reduce.2.cloned.1.call-start
  125.3 0.0 copy-done.2
  125.3 4.4 %fusion.10 = f32[2048,16]{0,1:T(8,128)} fusion(bf16[1536,16]{0,1:T(8,128)(2,1)S(1)} %copy-done.2, bf16[1536,2048]{1,0:T(8,128)(2,1)} %param.10), kind=kOutput, calls=%fused_computation.18 | convolution fusion | flops 100663296 | bytes 6471680 | tf_op jit(solution)/shard_map/dot_general | solution.py:50
  129.7 0.0 all-reduce.2.cloned.1.call-update
  129.7 0.0 all-gather.5.cloned.1.call-start
  129.8 1.1 copy.17
  130.8 15.4 %reduce-scatter.5.cloned.1.call-done = f32[32,256]{1,0:T(8,128)} async-done(((f32[32,1024]{1,0:T(8,128)}), f32[32,256]{1,0:T(8,128)}) %reduce-scatter.5.cloned.1.call-update) | async-done | bytes 32784 | tf_op jit(solution)/shard_map/reduce_scatter | solution.py:35
  146.3 1.4 add_divide_fusion
  147.7 30.8 %all_gather.10 = f32[256,256]{1,0:T(8,128)S(1)} all-gather(f32[32,256]{1,0:T(8,128)S(1)} %get-tuple-element.19), channel_id=1, replica_groups=mesh['fs'=8,'tp'=4] {'fs'}, dimensions={0}, use_global_device_ids=true | all-gather | bytes 294912 | tf_op jit(solution)/shard_map/all_gather | solution.py:68
  178.5 0.0 copy-done.1
  178.5 1.7 multiply_reduce_fusion
  180.2 38.8 %psum.14 = f32[]{:T(128)} all-reduce(f32[]{:T(128)} %get-tuple-element.24), channel_id=1, replica_groups=mesh['fs'=8,'tp'=4] {'fs','tp'}, use_global_device_ids=true, to_apply=%region_3.0 | all-reduce | flops 1 | bytes 8 | tf_op jit(solution)/shard_map/psum | solution.py:72
  219.7 1.8 fusion.6
  221.6 0.0 all-gather.5.cloned.1.call-update
  221.6 37.3 %all-reduce.2.cloned.1.call-done = f32[2048,16]{0,1:T(8,128)} async-done(((f32[2048,16]{0,1:T(8,128)}), f32[2048,16]{0,1:T(8,128)}) %all-reduce.2.cloned.1.call-update) | async-done | bytes 131088 | tf_op jit(solution)/shard_map/psum | solution.py:53
  258.9 1.9 subtract_convert_fusion.2
  260.7 1.8 copy.18
  262.5 1.8 copy.19
  264.3 0.0 all-gather.5.cloned.1.call-done
  264.3 2.3 copy.20
Async XLA Ops:
  8.0 51.0 %copy-start = (bf16[1536,1024]{1,0:T(8,128)(2,1)S(1)}, bf16[1536,1024]{1,0:T(8,128)(2,1)}, u32[]{:S(2)}) copy-start(bf16[1536,1024]{1,0:T(8,128)(2,1)} %param.11) | copy-start | bytes 9437188
  8.0 46.0 %all-gather.3.cloned.1.call-start = ((), (), s32[]{:S(2)}) async-start(), calls=%async_computation.2 | async-start | bytes 1179648 | tf_op jit(solution)/shard_map/all_gather | solution.py:59
  8.7 116.5 %reduce-scatter.3.cloned.1.call-start = ((), (), s32[]{:S(2)}) async-start(), calls=%async_computation.3 | async-start | bytes 1179648 | tf_op jit(solution)/shard_map/reduce_scatter | solution.py:34
  60.0 65.3 %copy-start.2 = (bf16[1536,16]{0,1:T(8,128)(2,1)S(1)}, bf16[1536,16]{0,1:T(8,128)(2,1)}, u32[]{:S(2)}) copy-start(bf16[1536,16]{0,1:T(8,128)(2,1)} %param.12) | copy-start | bytes 147460
  62.1 84.2 %reduce-scatter.5.cloned.1.call-start = ((), (), s32[]{:S(2)}) async-start(), calls=%async_computation.4 | async-start | bytes 163840 | tf_op jit(solution)/shard_map/reduce_scatter | solution.py:35
  125.2 53.3 %copy-start.1 = (bf16[256,256]{1,0:T(8,128)(2,1)S(1)}, bf16[256,256]{1,0:T(8,128)(2,1)}, u32[]{:S(2)}) copy-start(bf16[256,256]{1,0:T(8,128)(2,1)} %param.14) | copy-start | bytes 393220
  125.2 133.6 %all-reduce.2.cloned.1.call-start = ((), (), s32[]{:S(2)}) async-start(), calls=%async_computation.6 | async-start | bytes 262144 | tf_op jit(solution)/shard_map/psum | solution.py:53
  129.7 134.6 %all-gather.5.cloned.1.call-start = ((), (), s32[]{:S(2)}) async-start(), calls=%async_computation.5 | async-start | bytes 1179648 | tf_op jit(solution)/shard_map/all_gather | solution.py:75
Sparse Core Ops, SparseCore 0:
  10.9 42.9 all-gather.2
  62.2 62.9 reduce-scatter.2
  127.6 18.6 reduce-scatter.4
  221.7 41.0 all-gather.4
Sparse Core Ops, SparseCore 1:
  131.9 127.0 all-reduce.1
where the time goes:
time: 274 us
  waiting for transfers between devices  162 us (59%)
  blocking collectives  69.6 us (25%)
  between operations  16 us (6%)
  matrix products  14.1 us (5%)
  local copies, waits for them, and re-layouts  6.93 us (3%)
  other arithmetic  5.11 us (2%)
    reduce_scatter x1, waiting for transfers between devices, block_sum(): row_block = lax.psum_scatter(result, 'fs', scatter_dimension=0, tiled=True)  63.1 us
    all_gather x1, waiting for transfers between devices, local(): lax.all_gather(value_factor, 'fs', axis=0, tiled=True)  45.2 us
    psum x1, blocking collectives, local(): squares = lax.psum(jnp.sum(raw_update * raw_update), ('fs', 'tp'))  38.8 us
    psum x1, waiting for transfers between devices, local(): decay_grad = lax.psum(decay_local, ('fs', 'tp'))  37.3 us
    all_gather x1, blocking collectives, local(): lax.all_gather(direction, 'fs', axis=0, tiled=True)  30.8 us
    reduce_scatter x1, waiting for transfers between devices, block_sum(): return lax.psum_scatter(row_block, 'tp', scatter_dimension=1, tiled=True)  15.4 us
    unnamed x10, local copies, waits for them, and re-layouts  6.93 us
  transfers between devices with their start and end apart: 5, of which 4 were waited for; matrix products, arithmetic and copies ran while one was open for 6% of the time, Pallas kernels for 0%

commit v1 on v0

v1 whole, which is shorter than its diff:
```python
import jax
import jax.numpy as jnp
from jax import lax
from jax.sharding import PartitionSpec as P

BETA_ONE = 0.9
BETA_TWO = 0.99
ADAM_EPS = 1e-08
RMS_EPS = 1e-06
LEARN_RATE = 0.05
TOKEN_DIMS = (((0,), (0,)), ((), ()))
F32 = jnp.float32
BF16 = jnp.bfloat16


def adam_direction(moment_one, moment_two, gradient):
    mean_new = BETA_ONE * moment_one + (1.0 - BETA_ONE) * gradient
    second_new = BETA_TWO * moment_two + (1.0 - BETA_TWO) * gradient * gradient
    return (mean_new, second_new, mean_new / (jnp.sqrt(second_new) + ADAM_EPS))


def split_two(wide):
    high = lax.optimization_barrier(wide.astype(BF16))
    low = (wide - high.astype(F32)).astype(BF16)
    return high, low


def swap(block, axis, bit):
    count = lax.axis_size(axis)
    return lax.ppermute(block, axis, [(i, i ^ bit) for i in range(count)])


def direct_gather(block, axis):
    count = lax.axis_size(axis)
    me = lax.axis_index(axis)
    parts = [block] + [
        lax.ppermute(block, axis, [(i, (i + step) % count) for i in range(count)])
        for step in range(1, count)
    ]
    out = jnp.zeros((count,) + block.shape, block.dtype)
    for step, part in enumerate(parts):
        out = lax.dynamic_update_index_in_dim(out, part, (me - step) % count, 0)
    return out


def xor_bits(count):
    bits, bit = [], 1
    while bit < count:
        bits.append(bit)
        bit *= 2
    assert bit == count
    return bits


def xor_reduce_scatter(pieces, axis):
    left = list(range(len(pieces)))
    for bit in xor_bits(len(pieces)):
        sent = [o for o in left if o & bit]
        left = [o for o in left if not o & bit]
        for o in sent:
            pieces[o ^ bit] = pieces[o ^ bit] + swap(pieces[o], axis, bit)
    return pieces[0]


def xor_gather(block, axis):
    found = [block]
    for bit in xor_bits(lax.axis_size(axis)):
        found = found + [swap(part, axis, bit) for part in found]
    return found


def local(
    saved_input,
    value_cotangent,
    decay_cotangent,
    value_master,
    value_factor,
    value_mean,
    value_second,
    decay_master,
    decay_mean,
    decay_second,
):
    fs_count, tp_count = lax.axis_size("fs"), lax.axis_size("tp")
    tp_me, fs_me = lax.axis_index("tp"), lax.axis_index("fs")
    width_in, rank = saved_input.shape[1], value_factor.shape[1]
    columns = value_cotangent.shape[1] // tp_count
    heads = decay_cotangent.shape[1]
    shard_rows = value_factor.shape[0]
    half_rows = shard_rows // 2
    core = tp_me % 2

    half = lax.dynamic_slice_in_dim(value_factor, core * half_rows, half_rows, 0)
    mine = direct_gather(half, "fs")
    other = swap(mine, "tp", 1)
    first = jnp.where(core == 0, mine, other)
    second = jnp.where(core == 0, other, mine)
    factor = jnp.stack([first, second], 1).reshape(width_in, rank)

    gradient = lax.dot_general(
        saved_input, value_cotangent, TOKEN_DIMS, preferred_element_type=F32
    )
    high, low = split_two(gradient)
    decay_local = lax.dot_general(
        decay_cotangent, saved_input, TOKEN_DIMS, preferred_element_type=F32
    )

    decay_width = width_in // tp_count
    pieces = []
    for offset in range(tp_count):
        member = tp_me ^ offset
        term = jnp.zeros((rank, columns), F32)
        for part in (high, low):
            block = lax.dynamic_slice_in_dim(part, member * columns, columns, 1)
            term = term + lax.dot_general(factor, block, TOKEN_DIMS, preferred_element_type=F32)
        decay_block = lax.dynamic_slice_in_dim(decay_local, member * decay_width, decay_width, 1)
        pieces.append(
            jnp.concatenate(
                [
                    term.reshape(fs_count, rank // fs_count, columns),
                    decay_block.reshape(fs_count, -1, columns),
                ],
                1,
            )
        )
    block_sum = xor_reduce_scatter(pieces, "tp")
    owned = jnp.sum(lax.all_to_all(block_sum, "fs", 0, 0, tiled=True), 0)
    rank_rows = rank // fs_count
    projected, decay_part = owned[:rank_rows], owned[rank_rows:]
    mean_new, second_new, direction = adam_direction(value_mean, value_second, projected)

    spread = direct_gather(jnp.concatenate([direction, decay_part], 0), "fs")
    direction_all = spread[:, :rank_rows].reshape(rank, columns)
    decay_block = spread[:, rank_rows:].reshape(heads, decay_width)

    parts = split_two(direction_all)
    raw_all = jnp.dot(factor, parts[0], preferred_element_type=F32) + jnp.dot(
        factor, parts[1], preferred_element_type=F32
    )
    squares = jnp.broadcast_to(jnp.sum(raw_all * raw_all), (8, 128))
    for bit in xor_bits(tp_count):
        squares = squares + swap(squares, "tp", bit)
    entries = width_in * value_cotangent.shape[1]
    scale = lax.rsqrt(squares[0, 0] / entries + RMS_EPS)
    raw_update = lax.dynamic_slice_in_dim(raw_all, fs_me * shard_rows, shard_rows, 0)
    value_step = raw_update * scale
    value_new = value_master - LEARN_RATE * value_step
    value_copy = direct_gather(value_new.astype(BF16), "fs").reshape(width_in, columns)

    decay_grad = jnp.zeros((heads, width_in), F32)
    for offset, part in enumerate(xor_gather(decay_block, "tp")):
        decay_grad = lax.dynamic_update_slice_in_dim(
            decay_grad, part, (tp_me ^ offset) * decay_width, 1
        )
    unused_mean, unused_second, decay_step = adam_direction(
        decay_mean, decay_second, decay_grad.T
    )
    decay_copy = (decay_master - LEARN_RATE * decay_step).astype(BF16)
    return (value_step, value_new, value_copy, mean_new, second_new, decay_step, decay_copy)


def solution(mesh):
    in_specs = (
        P(("fs", "tp"), None),
        P(("fs", "tp"), None),
        P(("fs", "tp"), None),
        P("fs", "tp"),
        P("fs", None),
        P("fs", "tp"),
        P("fs", "tp"),
        P(),
        P(),
        P(),
    )
    out_specs = (
        P("fs", "tp"),
        P("fs", "tp"),
        P(None, "tp"),
        P("fs", "tp"),
        P("fs", "tp"),
        P(),
        P(),
    )
    return jax.shard_map(local, mesh=mesh, in_specs=in_specs, out_specs=out_specs, check_vma=False)
```

time: 274 us -> 131 us (0.48)
  waiting for transfers between devices: 162 us -> 22.7 us
  blocking collectives: 69.6 us -> 13.1 us
  starting transfers between devices: 0.2 us -> 41.6 us
  between operations: 16 us -> 1.86 us
  other arithmetic: 5.11 us -> 14.2 us
  matrix products: 14.1 us -> 21.6 us
  local copies, waits for them, and re-layouts: 6.93 us -> 13.9 us
    reduce_scatter x2 -> x0, waiting for transfers between devices: 78.5 us -> none  [the longest x1 63.1 us: block_sum(): row_block = lax.psum_scatter(result, 'fs', scatter_dimension=0, tiled=True)]
    all_gather x2 -> x0, waiting for transfers between devices: 45.2 us -> none  [the longest x1 45.2 us: local(): lax.all_gather(value_factor, 'fs', axis=0, tiled=True)]
    ppermute x0 -> x30, starting transfers between devices: none -> 41.6 us  [the longest x21 36 us: direct_gather(): lax.ppermute(block, axis, [(i, (i + step) % count) for i in range(count)])]
    psum x1 -> x0, blocking collectives: 38.8 us -> none  [local(): squares = lax.psum(jnp.sum(raw_update * raw_update), ('fs', 'tp'))]
    psum x1 -> x0, waiting for transfers between devices: 37.3 us -> none  [local(): decay_grad = lax.psum(decay_local, ('fs', 'tp'))]
    all_gather x1 -> x0, blocking collectives: 30.8 us -> none  [local(): lax.all_gather(direction, 'fs', axis=0, tiled=True)]
    ppermute x0 -> x30, waiting for transfers between devices: none -> 22.7 us  [the longest x9 14.2 us: swap(): return lax.ppermute(block, axis, [(i, i ^ bit) for i in range(count)])]
    all_to_all x0 -> x1, blocking collectives: none -> 13.1 us  [local(): owned = jnp.sum(lax.all_to_all(block_sum, 'fs', 0, 0, tiled=True), 0)]
  transfers between devices with their start and end apart: 5 -> 30, of which waited for: 4 -> 12; matrix products, arithmetic and copies ran while one was open for 6% -> 28% of each run, Pallas kernels for 0% -> 0%
where the time goes in v1:
time: 131 us; the launch traced here: 129 us
  starting transfers between devices  41.6 us (32%)
  waiting for transfers between devices  22.7 us (17%)
  matrix products  21.6 us (16%)
  other arithmetic  14.2 us (11%)
  local copies, waits for them, and re-layouts  13.9 us (11%)
  blocking collectives  13.1 us (10%)
  between operations  1.86 us (1%)
    ppermute x21, starting transfers between devices, direct_gather(): lax.ppermute(block, axis, [(i, (i + step) % count) for i in range(count)])  36 us
    ppermute x9, waiting for transfers between devices, swap(): return lax.ppermute(block, axis, [(i, i ^ bit) for i in range(count)])  14.2 us
    all_to_all x1, blocking collectives, local(): owned = jnp.sum(lax.all_to_all(block_sum, 'fs', 0, 0, tiled=True), 0)  13.1 us
    dot_general x1, matrix products, local(): lax.dot_general(saved_input, value_cotangent, TOKEN_DIMS, preferred_eleme...  12.6 us
    dynamic_update_slice x22, local copies, waits for them, and re-layouts, direct_gather(): out = lax.dynamic_update_index_in_dim(out, part, (me - step) % count, 0)  9.67 us
    ppermute x21, waiting for transfers between devices, direct_gather(): lax.ppermute(block, axis, [(i, (i + step) % count) for i in range(count)])  8.45 us
    convert_element_type x2, other arithmetic, split_two(): low = (wide - high.astype(F32)).astype(BF16)  6.22 us
    ppermute x9, starting transfers between devices, swap(): return lax.ppermute(block, axis, [(i, i ^ bit) for i in range(count)])  5.66 us
  transfers between devices with their start and end apart: 30, of which 12 were waited for; matrix products, arithmetic and copies ran while one was open for 28% of the time, Pallas kernels for 0%

profile of v1, /device:TPU:0, one launch (start us, length us, event | category | flops | bytes accessed | tf_op | source)
XLA Modules:
  0.0 129.0 jit_solution(11814154798816951165)
XLA Ops:
  0.7 0.8 broadcast_in_dim.90
  1.5 1.7 %bitcast_dynamic-update-slice_fusion.15 = (bf16[8,128,256]{2,1,0:T(8,128)(2,1)}, bf16[128,256]{1,0:T(8,128)(2,1)S(1)}) fusion(bf16[8,128,256]{2,1,0:T(8,128)(2,1)} %broadcast_in_dim.90, s32[]{:T(128)S(6)} %select_n.168, bf16[256,256]{1,0:T(8,128)(2,1)} %param.14, s32[]{:T(128)S(6)} %select_n.166), kind=kLoop, calls=%fused_computation.55 | loop fusion | bytes 196616 | tf_op jit(solution)/shard_map/jit(dynamic_update_index_in_dim)/dynamic_update_slice | solution.py:42
  3.2 3.0 %collective-permute-start = (bf16[128,256]{1,0:T(8,128)(2,1)S(1)}, bf16[128,256]{1,0:T(8,128)(2,1)}, u32[]{:S(2)}, u32[]{:S(2)}) collective-permute-start(bf16[128,256]{1,0:T(8,128)(2,1)S(1)} %get-tuple-element.17), channel_id=1, source_target_pairs={{0,4},{4,8},{8,12},{12,16},{16,20},{20,24},{24,28},{28,0},{1,5},{5... | collective-permute-start | bytes 196616 | tf_op jit(solution)/shard_map/ppermute | solution.py:37
  6.2 1.6 %collective-permute-start.1 = (bf16[128,256]{1,0:T(8,128)(2,1)S(1)}, bf16[128,256]{1,0:T(8,128)(2,1)}, u32[]{:S(2)}, u32[]{:S(2)}) collective-permute-start(bf16[128,256]{1,0:T(8,128)(2,1)S(1)} %get-tuple-element.17), channel_id=1, source_target_pairs={{0,8},{4,12},{8,16},{12,20},{16,24},{20,28},{24,0},{28,4},{1,9},{5... | collective-permute-start | bytes 196616 | tf_op jit(solution)/shard_map/ppermute | solution.py:37
  7.8 2.6 %collective-permute-start.2 = (bf16[128,256]{1,0:T(8,128)(2,1)S(1)}, bf16[128,256]{1,0:T(8,128)(2,1)}, u32[]{:S(2)}, u32[]{:S(2)}) collective-permute-start(bf16[128,256]{1,0:T(8,128)(2,1)S(1)} %get-tuple-element.17), channel_id=1, source_target_pairs={{0,12},{4,16},{8,20},{12,24},{16,28},{20,0},{24,4},{28,8},{1,13},{... | collective-permute-start | bytes 196616 | tf_op jit(solution)/shard_map/ppermute | solution.py:37
  10.4 1.2 collective-permute-start.3
  11.6 2.6 %collective-permute-start.4 = (bf16[128,256]{1,0:T(8,128)(2,1)S(1)}, bf16[128,256]{1,0:T(8,128)(2,1)S(1)}, u32[]{:S(2)}, u32[]{:S(2)}) collective-permute-start(bf16[128,256]{1,0:T(8,128)(2,1)S(1)} %get-tuple-element.17), channel_id=1, source_target_pairs={{0,20},{4,24},{8,28},{12,0},{16,4},{20,8},{24,12},{28,16},{1,21},{... | collective-permute-start | bytes 196616 | tf_op jit(solution)/shard_map/ppermute | solution.py:37
  14.2 12.6 %fusion.30 = (bf16[2048,1024]{1,0:T(8,128)(2,1)}, f32[2048,1024]{1,0:T(8,128)}) fusion(bf16[1536,2048]{1,0:T(8,128)(2,1)} %param.10, bf16[1536,1024]{1,0:T(8,128)(2,1)S(1)} %copy-done), kind=kOutput, calls=%fused_computation.87 | convolution fusion | flops 6444548096 | bytes 22020096 | tf_op jit(solution)/shard_map/dot_general | solution.py:100
  26.8 0.9 fusion.31
  27.9 1.4 %collective-permute-start.5 = (bf16[128,256]{1,0:T(8,128)(2,1)S(1)}, bf16[128,256]{1,0:T(8,128)(2,1)S(1)}, u32[]{:S(2)}, u32[]{:S(2)}) collective-permute-start(bf16[128,256]{1,0:T(8,128)(2,1)S(1)} %get-tuple-element.17), channel_id=1, source_target_pairs={{0,24},{4,28},{8,0},{12,4},{16,8},{20,12},{24,16},{28,20},{1,25},{... | collective-permute-start | bytes 196616 | tf_op jit(solution)/shard_map/ppermute | solution.py:37
  29.3 1.5 %bitcast_dynamic-update-slice_fusion.14 = bf16[8,128,256]{2,1,0:T(8,128)(2,1)} fusion(bf16[8,128,256]{2,1,0:T(8,128)(2,1)} %get-tuple-element.16, s32[]{:T(128)S(6)} %select_n.170, bf16[128,256]{1,0:T(8,128)(2,1)} %collective-permute-done), kind=kLoop, calls=%fused_computation.54 | loop fusion | bytes 131076 | tf_op jit(solution)/shard_map/jit(dynamic_update_index_in_dim)/dynamic_update_slice | solution.py:42
  30.8 1.4 %collective-permute-start.6 = (bf16[128,256]{1,0:T(8,128)(2,1)S(1)}, bf16[128,256]{1,0:T(8,128)(2,1)S(1)}, u32[]{:S(2)}, u32[]{:S(2)}) collective-permute-start(bf16[128,256]{1,0:T(8,128)(2,1)S(1)} %get-tuple-element.17), channel_id=1, source_target_pairs={{0,28},{4,0},{8,4},{12,8},{16,12},{20,16},{24,20},{28,24},{1,29},{... | collective-permute-start | bytes 196616 | tf_op jit(solution)/shard_map/ppermute | solution.py:37
  32.2 1.5 %bitcast_dynamic-update-slice_fusion.13 = bf16[8,128,256]{2,1,0:T(8,128)(2,1)} fusion(bf16[8,128,256]{2,1,0:T(8,128)(2,1)} %bitcast_dynamic-update-slice_fusion.14, s32[]{:T(128)S(6)} %select_n.172, bf16[128,256]{1,0:T(8,128)(2,1)} %collective-permute-done.1), kind=kLoop, calls=%fused_computation.53 | loop fusion | bytes 131076 | tf_op jit(solution)/shard_map/jit(dynamic_update_index_in_dim)/dynamic_update_slice | solution.py:42
  33.7 1.5 %bitcast_dynamic-update-slice_fusion.12 = bf16[8,128,256]{2,1,0:T(8,128)(2,1)} fusion(bf16[8,128,256]{2,1,0:T(8,128)(2,1)} %bitcast_dynamic-update-slice_fusion.13, s32[]{:T(128)S(6)} %select_n.174, bf16[128,256]{1,0:T(8,128)(2,1)} %collective-permute-done.2), kind=kLoop, calls=%fused_computation.52 | loop fusion | bytes 131076 | tf_op jit(solution)/shard_map/jit(dynamic_update_index_in_dim)/dynamic_update_slice | solution.py:42
  35.2 1.5 %bitcast_dynamic-update-slice_fusion.11 = bf16[8,128,256]{2,1,0:T(8,128)(2,1)} fusion(bf16[8,128,256]{2,1,0:T(8,128)(2,1)} %bitcast_dynamic-update-slice_fusion.12, s32[]{:T(128)S(6)} %select_n.176, bf16[128,256]{1,0:T(8,128)(2,1)} %collective-permute-done.3), kind=kLoop, calls=%fused_computation.51 | loop fusion | bytes 131076 | tf_op jit(solution)/shard_map/jit(dynamic_update_index_in_dim)/dynamic_update_slice | solution.py:42
  38.6 6.2 %subtract_convert_fusion = bf16[2048,1024]{1,0:T(8,128)(2,1)S(1)} fusion(f32[2048,1024]{1,0:T(8,128)} %get-tuple-element.25, bf16[2048,1024]{1,0:T(8,128)(2,1)} %get-tuple-element.24), kind=kLoop, calls=%fused_computation | loop fusion | flops 6291456 | bytes 16777216 | tf_op jit(solution)/shard_map/convert_element_type | solution.py:24
  44.8 1.3 select_bitcast_fusion.1
  46.2 0.9 copy-done.3
  51.5 1.6 %collective-permute-start.10 = (f32[8,36,256]{2,1,0:T(8,128)S(1)}, f32[8,36,256]{2,1,0:T(8,128)S(1)}, u32[]{:S(2)}, u32[]{:S(2)}) collective-permute-start(f32[8,36,256]{2,1,0:T(8,128)S(1)} %maximum_add_fusion.1), channel_id=1, source_target_pairs={{0,2},{1,3},{2,0},{3,1},{4,6},{5,7},{6,4},{7,5},{8,10},{9,11},{10,... | collective-permute-start | bytes 884744 | tf_op jit(solution)/shard_map/ppermute | solution.py:30
  54.0 7.2 %collective-permute-done.10 = f32[8,36,256]{2,1,0:T(8,128)S(1)} collective-permute-done((f32[8,36,256]{2,1,0:T(8,128)S(1)}, f32[8,36,256]{2,1,0:T(8,128)S(1)}, u32[]{:S(2)}, u32[]{:S(2)}) %collective-permute-start.10) | collective-permute-done | bytes 294944 | tf_op jit(solution)/shard_map/ppermute | solution.py:30
  61.3 13.1 %all_to_all.5 = f32[8,36,256]{2,1,0:T(8,128)S(1)} all-to-all(f32[8,36,256]{2,1,0:T(8,128)S(1)} %fusion.12), channel_id=1, replica_groups=mesh['fs'=8,'tp'=4] {'fs'}, dimensions={0} | all-to-all | bytes 589824 | tf_op jit(solution)/shard_map/all_to_all | solution.py:127
  74.5 1.5 %add_divide_fusion = (f32[32,256]{1,0:T(8,128)S(1)}, f32[32,256]{1,0:T(8,128)}, f32[32,256]{1,0:T(8,128)}) fusion(f32[36,256]{1,0:T(8,128)S(1)} %reduce_sum.18, f32[32,256]{1,0:T(8,128)S(1)} %copy-done.7, f32[32,256]{1,0:T(8,128)} %param.15), kind=kLoop, calls=%fused_computation.67 | loop fusion | flops 73728 | bytes 196608 | tf_op jit(solution)/shard_map/div | solution.py:19
  76.0 0.9 collective-permute-start.11
  77.2 2.2 %collective-permute-start.13 = (f32[36,256]{1,0:T(8,128)S(1)}, f32[36,256]{1,0:T(8,128)S(1)}, u32[]{:S(2)}, u32[]{:S(2)}) collective-permute-start(f32[36,256]{1,0:T(8,128)S(1)} %pad_maximum_fusion.3), channel_id=1, source_target_pairs={{0,12},{4,16},{8,20},{12,24},{16,28},{20,0},{24,4},{28,8},{1,13},{... | collective-permute-start | bytes 110600 | tf_op jit(solution)/shard_map/ppermute | solution.py:37
  79.4 2.6 %collective-permute-start.14 = (f32[36,256]{1,0:T(8,128)S(1)}, f32[36,256]{1,0:T(8,128)S(1)}, u32[]{:S(2)}, u32[]{:S(2)}) collective-permute-start(f32[36,256]{1,0:T(8,128)S(1)} %pad_maximum_fusion.3), channel_id=1, source_target_pairs={{0,16},{4,20},{8,24},{12,28},{16,0},{20,4},{24,8},{28,12},{1,17},{... | collective-permute-start | bytes 110600 | tf_op jit(solution)/shard_map/ppermute | solution.py:37
  83.0 1.6 %collective-permute-start.16 = (f32[36,256]{1,0:T(8,128)S(1)}, f32[36,256]{1,0:T(8,128)S(1)}, u32[]{:S(2)}, u32[]{:S(2)}) collective-permute-start(f32[36,256]{1,0:T(8,128)S(1)} %pad_maximum_fusion.3), channel_id=1, source_target_pairs={{0,24},{4,28},{8,0},{12,4},{16,8},{20,12},{24,16},{28,20},{1,25},{... | collective-permute-start | bytes 110600 | tf_op jit(solution)/shard_map/ppermute | solution.py:37
  84.6 2.1 %collective-permute-start.17 = (f32[36,256]{1,0:T(8,128)S(1)}, f32[36,256]{1,0:T(8,128)S(1)}, u32[]{:S(2)}, u32[]{:S(2)}) collective-permute-start(f32[36,256]{1,0:T(8,128)S(1)} %pad_maximum_fusion.3), channel_id=1, source_target_pairs={{0,28},{4,0},{8,4},{12,8},{16,12},{20,16},{24,20},{28,24},{1,29},{... | collective-permute-start | bytes 110600 | tf_op jit(solution)/shard_map/ppermute | solution.py:37
  87.5 1.3 %collective-permute-done.17 = f32[36,256]{1,0:T(8,128)S(1)} collective-permute-done((f32[36,256]{1,0:T(8,128)S(1)}, f32[36,256]{1,0:T(8,128)S(1)}, u32[]{:S(2)}, u32[]{:S(2)}) %collective-permute-start.17) | collective-permute-done | bytes 36896 | tf_op jit(solution)/shard_map/ppermute | solution.py:37
  88.9 1.7 %fusion.32 = f32[2048,256]{1,0:T(8,128)S(1)} fusion(bf16[2048,256]{1,0:T(8,128)(2,1)} %bitcast.98, bf16[256,256]{1,0:T(8,128)(2,1)S(1)} %bitcast_convert_fusion), kind=kOutput, calls=%fused_computation.89 | convolution fusion | flops 268435456 | bytes 3276800 | tf_op jit(solution)/shard_map/dot_general | solution.py:137
  90.6 2.6 %multiply_reduce_fusion = (f32[]{:T(128)}, f32[2048,256]{1,0:T(8,128)}) fusion(f32[2048,256]{1,0:T(8,128)S(1)} %fusion.32, bf16[2048,256]{1,0:T(8,128)(2,1)S(1)} %bitcast.99, bf16[256,256]{1,0:T(8,128)(2,1)S(1)} %fusion.13), kind=kOutput, calls=%fused_computation.2 | convolution fusion | flops 270008320 | bytes 5373956 | tf_op jit(solution)/shard_map/dot_general | solution.py:137
  94.5 1.5 %collective-permute-start.28 = (f32[16,512]{1,0:T(8,128)S(1)}, f32[16,512]{1,0:T(8,128)S(1)}, u32[]{:S(2)}, u32[]{:S(2)}) collective-permute-start(f32[16,512]{1,0:T(8,128)S(1)} %reshape.66), channel_id=1, source_target_pairs={{0,2},{1,3},{2,0},{3,1},{4,6},{5,7},{6,4},{7,5},{8,10},{9,11},{10,... | collective-permute-start | bytes 98312 | tf_op jit(solution)/shard_map/ppermute | solution.py:30
  96.0 0.6 broadcast_add_fusion
  97.4 3.0 %collective-permute-done.19 = f32[8,128]{1,0:T(8,128)S(1)} collective-permute-done((f32[8,128]{1,0:T(8,128)S(1)}, f32[8,128]{1,0:T(8,128)S(1)}, u32[]{:S(2)}, u32[]{:S(2)}) %collective-permute-start.19) | collective-permute-done | bytes 4128 | tf_op jit(solution)/shard_map/ppermute | solution.py:30
  100.4 0.6 fusion.49
  102.3 1.9 %bitcast_dynamic-update-slice_fusion.7 = (bf16[8,256,256]{2,1,0:T(8,128)(2,1)S(1)}, bf16[256,256]{1,0:T(8,128)(2,1)S(1)}, f32[256,256]{1,0:T(8,128)}, f32[256,256]{1,0:T(8,128)}) fusion(bf16[8,256,256]{2,1,0:T(8,128)(2,1)S(1)} %broadcast_in_dim.109, s32[]{:T(128)S(6)} %select_n.168, f32[256,256]{1,0:T(8,128)} %param.13, f32[]{:T(128)} %bitcast.25, ...), kind=kLoop, calls=%fused_computation.46 | loop fusion | flops 262144 | bytes 1310732 | tf_op jit(solution)/shard_map/jit(dynamic_update_index_in_dim)/dynamic_update_slice | solution.py:42
  104.2 2.1 %collective-permute-start.20 = (bf16[256,256]{1,0:T(8,128)(2,1)S(1)}, bf16[256,256]{1,0:T(8,128)(2,1)S(1)}, u32[]{:S(2)}, u32[]{:S(2)}) collective-permute-start(bf16[256,256]{1,0:T(8,128)(2,1)S(1)} %get-tuple-element.10), channel_id=1, source_target_pairs={{0,4},{4,8},{8,12},{12,16},{16,20},{20,24},{24,28},{28,0},{1,5},{5... | collective-permute-start | bytes 393224 | tf_op jit(solution)/shard_map/ppermute | solution.py:37
  106.3 2.0 %collective-permute-start.21 = (bf16[256,256]{1,0:T(8,128)(2,1)S(1)}, bf16[256,256]{1,0:T(8,128)(2,1)S(1)}, u32[]{:S(2)}, u32[]{:S(2)}) collective-permute-start(bf16[256,256]{1,0:T(8,128)(2,1)S(1)} %get-tuple-element.10), channel_id=1, source_target_pairs={{0,8},{4,12},{8,16},{12,20},{16,24},{20,28},{24,0},{28,4},{1,9},{5... | collective-permute-start | bytes 393224 | tf_op jit(solution)/shard_map/ppermute | solution.py:37
  108.4 2.3 %collective-permute-start.23 = (bf16[256,256]{1,0:T(8,128)(2,1)S(1)}, bf16[256,256]{1,0:T(8,128)(2,1)S(1)}, u32[]{:S(2)}, u32[]{:S(2)}) collective-permute-start(bf16[256,256]{1,0:T(8,128)(2,1)S(1)} %get-tuple-element.10), channel_id=1, source_target_pairs={{0,16},{4,20},{8,24},{12,28},{16,0},{20,4},{24,8},{28,12},{1,17},{... | collective-permute-start | bytes 393224 | tf_op jit(solution)/shard_map/ppermute | solution.py:37
  111.3 3.4 %collective-permute-done.29 = f32[16,512]{1,0:T(8,128)S(1)} collective-permute-done((f32[16,512]{1,0:T(8,128)S(1)}, f32[16,512]{1,0:T(8,128)S(1)}, u32[]{:S(2)}, u32[]{:S(2)}) %collective-permute-start.29) | collective-permute-done | bytes 32800 | tf_op jit(solution)/shard_map/ppermute | solution.py:30
  114.7 3.0 %collective-permute-start.24 = (bf16[256,256]{1,0:T(8,128)(2,1)S(1)}, bf16[256,256]{1,0:T(8,128)(2,1)S(1)}, u32[]{:S(2)}, u32[]{:S(2)}) collective-permute-start(bf16[256,256]{1,0:T(8,128)(2,1)S(1)} %get-tuple-element.10), channel_id=1, source_target_pairs={{0,20},{4,24},{8,28},{12,0},{16,4},{20,8},{24,12},{28,16},{1,21},{... | collective-permute-start | bytes 393224 | tf_op jit(solution)/shard_map/ppermute | solution.py:37
  117.7 1.8 %subtract_convert_fusion.1 = (bf16[2048,16]{0,1:T(8,128)(2,1)}, f32[2048,16]{0,1:T(8,128)}) fusion(f32[2048,16]{0,1:T(8,128)} %param.17, f32[2048,16]{0,1:T(8,128)} %param.19, f32[16,2048]{1,0:T(8,128)S(1)} %constant_dynamic-update-slice_fusion, f32[2048,16]{0,1:T(8,128)} %param.18), kind=kLoop, calls=%fused_computation.47 | loop fusion | flops 393216 | bytes 720896 | tf_op jit(solution)/shard_map/convert_element_type | solution.py:158
  119.5 0.8 collective-permute-start.25
  120.3 1.5 %collective-permute-start.26 = (bf16[256,256]{1,0:T(8,128)(2,1)S(1)}, bf16[256,256]{1,0:T(8,128)(2,1)S(1)}, u32[]{:S(2)}, u32[]{:S(2)}) collective-permute-start(bf16[256,256]{1,0:T(8,128)(2,1)S(1)} %get-tuple-element.10), channel_id=1, source_target_pairs={{0,28},{4,0},{8,4},{12,8},{16,12},{20,16},{24,20},{28,24},{1,29},{... | collective-permute-start | bytes 393224 | tf_op jit(solution)/shard_map/ppermute | solution.py:37
  121.9 0.6 collective-permute-done.22
  122.5 0.7 collective-permute-done.23
  123.3 2.9 %collective-permute-done.24 = bf16[256,256]{1,0:T(8,128)(2,1)S(1)} collective-permute-done((bf16[256,256]{1,0:T(8,128)(2,1)S(1)}, bf16[256,256]{1,0:T(8,128)(2,1)S(1)}, u32[]{:S(2)}, u32[]{:S(2)}) %collective-permute-start.24) | collective-permute-done | bytes 131104 | tf_op jit(solution)/shard_map/ppermute | solution.py:37
  126.2 1.8 %collective-permute-done.25 = bf16[256,256]{1,0:T(8,128)(2,1)S(1)} collective-permute-done((bf16[256,256]{1,0:T(8,128)(2,1)S(1)}, bf16[256,256]{1,0:T(8,128)(2,1)S(1)}, u32[]{:S(2)}, u32[]{:S(2)}) %collective-permute-start.25) | collective-permute-done | bytes 131104 | tf_op jit(solution)/shard_map/ppermute | solution.py:37
  128.0 1.0 copy-done.5
  (99 shorter events, 12.9 us)
Async XLA Ops:
  0.6 13.6 %copy-start = (bf16[1536,1024]{1,0:T(8,128)(2,1)S(1)}, bf16[1536,1024]{1,0:T(8,128)(2,1)}, u32[]{:S(2)}) copy-start(bf16[1536,1024]{1,0:T(8,128)(2,1)} %param.11) | copy-start | bytes 9437188
  3.2 24.7 %collective-permute-start = (bf16[128,256]{1,0:T(8,128)(2,1)S(1)}, bf16[128,256]{1,0:T(8,128)(2,1)}, u32[]{:S(2)}, u32[]{:S(2)}) collective-permute-start(bf16[128,256]{1,0:T(8,128)(2,1)S(1)} %get-tuple-element.17), channel_id=1, source_target_pairs={{0,4},{4,8},{8,12},{12,16},{16,20},{20,24},{24,28},{28,0},{1,5},{5... | collective-permute-start | bytes 196616 | tf_op jit(solution)/shard_map/ppermute | solution.py:37
  6.2 24.6 %collective-permute-start.1 = (bf16[128,256]{1,0:T(8,128)(2,1)S(1)}, bf16[128,256]{1,0:T(8,128)(2,1)}, u32[]{:S(2)}, u32[]{:S(2)}) collective-permute-start(bf16[128,256]{1,0:T(8,128)(2,1)S(1)} %get-tuple-element.17), channel_id=1, source_target_pairs={{0,8},{4,12},{8,16},{12,20},{16,24},{20,28},{24,0},{28,4},{1,9},{5... | collective-permute-start | bytes 196616 | tf_op jit(solution)/shard_map/ppermute | solution.py:37
  7.8 25.9 %collective-permute-start.2 = (bf16[128,256]{1,0:T(8,128)(2,1)S(1)}, bf16[128,256]{1,0:T(8,128)(2,1)}, u32[]{:S(2)}, u32[]{:S(2)}) collective-permute-start(bf16[128,256]{1,0:T(8,128)(2,1)S(1)} %get-tuple-element.17), channel_id=1, source_target_pairs={{0,12},{4,16},{8,20},{12,24},{16,28},{20,0},{24,4},{28,8},{1,13},{... | collective-permute-start | bytes 196616 | tf_op jit(solution)/shard_map/ppermute | solution.py:37
  10.4 24.8 %collective-permute-start.3 = (bf16[128,256]{1,0:T(8,128)(2,1)S(1)}, bf16[128,256]{1,0:T(8,128)(2,1)}, u32[]{:S(2)}, u32[]{:S(2)}) collective-permute-start(bf16[128,256]{1,0:T(8,128)(2,1)S(1)} %get-tuple-element.17), channel_id=1, source_target_pairs={{0,16},{4,20},{8,24},{12,28},{16,0},{20,4},{24,8},{28,12},{1,17},{... | collective-permute-start | bytes 196616 | tf_op jit(solution)/shard_map/ppermute | solution.py:37
  11.6 25.1 %collective-permute-start.4 = (bf16[128,256]{1,0:T(8,128)(2,1)S(1)}, bf16[128,256]{1,0:T(8,128)(2,1)S(1)}, u32[]{:S(2)}, u32[]{:S(2)}) collective-permute-start(bf16[128,256]{1,0:T(8,128)(2,1)S(1)} %get-tuple-element.17), channel_id=1, source_target_pairs={{0,20},{4,24},{8,28},{12,0},{16,4},{20,8},{24,12},{28,16},{1,21},{... | collective-permute-start | bytes 196616 | tf_op jit(solution)/shard_map/ppermute | solution.py:37
  14.2 12.6 %copy-start.4 = (bf16[1536,2048]{1,0:T(8,128)(2,1)S(1)}, bf16[1536,2048]{1,0:T(8,128)(2,1)}, u32[]{:S(2)}) copy-start(bf16[1536,2048]{1,0:T(8,128)(2,1)} %param.10) | copy-start | bytes 18874372
  14.2 12.6 %copy-start.6 = (bf16[1536,16]{0,1:T(8,128)(2,1)S(1)}, bf16[1536,16]{0,1:T(8,128)(2,1)}, u32[]{:S(2)}) copy-start(bf16[1536,16]{0,1:T(8,128)(2,1)} %param.12) | copy-start | bytes 147460
  27.9 9.4 %collective-permute-start.5 = (bf16[128,256]{1,0:T(8,128)(2,1)S(1)}, bf16[128,256]{1,0:T(8,128)(2,1)S(1)}, u32[]{:S(2)}, u32[]{:S(2)}) collective-permute-start(bf16[128,256]{1,0:T(8,128)(2,1)S(1)} %get-tuple-element.17), channel_id=1, source_target_pairs={{0,24},{4,28},{8,0},{12,4},{16,8},{20,12},{24,16},{28,20},{1,25},{... | collective-permute-start | bytes 196616 | tf_op jit(solution)/shard_map/ppermute | solution.py:37
  30.8 7.1 %collective-permute-start.6 = (bf16[128,256]{1,0:T(8,128)(2,1)S(1)}, bf16[128,256]{1,0:T(8,128)(2,1)S(1)}, u32[]{:S(2)}, u32[]{:S(2)}) collective-permute-start(bf16[128,256]{1,0:T(8,128)(2,1)S(1)} %get-tuple-element.17), channel_id=1, source_target_pairs={{0,28},{4,0},{8,4},{12,8},{16,12},{20,16},{24,20},{28,24},{1,29},{... | collective-permute-start | bytes 196616 | tf_op jit(solution)/shard_map/ppermute | solution.py:37
  38.6 6.2 %collective-permute-start.7 = (bf16[8,128,256]{2,1,0:T(8,128)(2,1)}, bf16[8,128,256]{2,1,0:T(8,128)(2,1)S(1)}, u32[]{:S(2)}, u32[]{:S(2)}) collective-permute-start(bf16[8,128,256]{2,1,0:T(8,128)(2,1)} %bitcast_dynamic-update-slice_fusion.8), channel_id=1, source_target_pairs={{0,1},{1,0},{2,3},{3,2},{4,5},{5,4},{6,7},{7,6},{8,9},{9,8},{10,11... | collective-permute-start | bytes 1572872 | tf_op jit(solution)/shard_map/ppermute | solution.py:30
  44.8 2.3 %copy-start.3 = (bf16[2048,1024]{1,0:T(8,128)(2,1)S(1)}, bf16[2048,1024]{1,0:T(8,128)(2,1)}, u32[]{:S(2)}) copy-start(bf16[2048,1024]{1,0:T(8,128)(2,1)} %get-tuple-element.24) | copy-start | bytes 12582916
  46.2 7.4 %copy-start.1 = (bf16[8,2,128,256]{3,2,1,0:T(8,128)(2,1)}, bf16[8,2,128,256]{3,2,1,0:T(8,128)(2,1)S(1)}, u32[]{:S(2)}) copy-start(bf16[8,2,128,256]{3,2,1,0:T(8,128)(2,1)S(1)} %pad_maximum_fusion) | copy-start | bytes 3145732
  48.1 5.9 %collective-permute-start.8 = (f32[8,36,256]{2,1,0:T(8,128)S(1)}, f32[8,36,256]{2,1,0:T(8,128)S(1)}, u32[]{:S(2)}, u32[]{:S(2)}) collective-permute-start(f32[8,36,256]{2,1,0:T(8,128)S(1)} %pad_maximum_fusion.1), channel_id=1, source_target_pairs={{0,1},{1,0},{2,3},{3,2},{4,5},{5,4},{6,7},{7,6},{8,9},{9,8},{10,11... | collective-permute-start | bytes 884744 | tf_op jit(solution)/shard_map/ppermute | solution.py:30
  49.7 1.7 %collective-permute-start.9 = (f32[8,36,256]{2,1,0:T(8,128)S(1)}, f32[8,36,256]{2,1,0:T(8,128)S(1)}, u32[]{:S(2)}, u32[]{:S(2)}) collective-permute-start(f32[8,36,256]{2,1,0:T(8,128)S(1)} %pad_maximum_fusion.2), channel_id=1, source_target_pairs={{0,1},{1,0},{2,3},{3,2},{4,5},{5,4},{6,7},{7,6},{8,9},{9,8},{10,11... | collective-permute-start | bytes 884744 | tf_op jit(solution)/shard_map/ppermute | solution.py:30
  50.8 23.6 %copy-start.7 = (f32[32,256]{1,0:T(8,128)S(1)}, f32[32,256]{1,0:T(8,128)}, u32[]{:S(2)}) copy-start(f32[32,256]{1,0:T(8,128)} %param.16) | copy-start | bytes 98308
  51.5 9.8 %collective-permute-start.10 = (f32[8,36,256]{2,1,0:T(8,128)S(1)}, f32[8,36,256]{2,1,0:T(8,128)S(1)}, u32[]{:S(2)}, u32[]{:S(2)}) collective-permute-start(f32[8,36,256]{2,1,0:T(8,128)S(1)} %maximum_add_fusion.1), channel_id=1, source_target_pairs={{0,2},{1,3},{2,0},{3,1},{4,6},{5,7},{6,4},{7,5},{8,10},{9,11},{10,... | collective-permute-start | bytes 884744 | tf_op jit(solution)/shard_map/ppermute | solution.py:30
  74.4 16.1 %copy-start.2 = (bf16[8,2,128,256]{3,2,1,0:T(8,128)(2,1)S(1)}, bf16[8,2,128,256]{3,2,1,0:T(8,128)(2,1)}, u32[]{:S(2)}) copy-start(bf16[8,2,128,256]{3,2,1,0:T(8,128)(2,1)} %copy-done.1) | copy-start | bytes 3145732
  76.0 7.0 %collective-permute-start.11 = (f32[36,256]{1,0:T(8,128)S(1)}, f32[36,256]{1,0:T(8,128)S(1)}, u32[]{:S(2)}, u32[]{:S(2)}) collective-permute-start(f32[36,256]{1,0:T(8,128)S(1)} %pad_maximum_fusion.3), channel_id=1, source_target_pairs={{0,4},{4,8},{8,12},{12,16},{16,20},{20,24},{24,28},{28,0},{1,5},{5... | collective-permute-start | bytes 110600 | tf_op jit(solution)/shard_map/ppermute | solution.py:37
  76.8 7.8 %collective-permute-start.12 = (f32[36,256]{1,0:T(8,128)S(1)}, f32[36,256]{1,0:T(8,128)S(1)}, u32[]{:S(2)}, u32[]{:S(2)}) collective-permute-start(f32[36,256]{1,0:T(8,128)S(1)} %pad_maximum_fusion.3), channel_id=1, source_target_pairs={{0,8},{4,12},{8,16},{12,20},{16,24},{20,28},{24,0},{28,4},{1,9},{5... | collective-permute-start | bytes 110600 | tf_op jit(solution)/shard_map/ppermute | solution.py:37
  77.2 9.5 %collective-permute-start.13 = (f32[36,256]{1,0:T(8,128)S(1)}, f32[36,256]{1,0:T(8,128)S(1)}, u32[]{:S(2)}, u32[]{:S(2)}) collective-permute-start(f32[36,256]{1,0:T(8,128)S(1)} %pad_maximum_fusion.3), channel_id=1, source_target_pairs={{0,12},{4,16},{8,20},{12,24},{16,28},{20,0},{24,4},{28,8},{1,13},{... | collective-permute-start | bytes 110600 | tf_op jit(solution)/shard_map/ppermute | solution.py:37
  79.4 7.3 %collective-permute-start.14 = (f32[36,256]{1,0:T(8,128)S(1)}, f32[36,256]{1,0:T(8,128)S(1)}, u32[]{:S(2)}, u32[]{:S(2)}) collective-permute-start(f32[36,256]{1,0:T(8,128)S(1)} %pad_maximum_fusion.3), channel_id=1, source_target_pairs={{0,16},{4,20},{8,24},{12,28},{16,0},{20,4},{24,8},{28,12},{1,17},{... | collective-permute-start | bytes 110600 | tf_op jit(solution)/shard_map/ppermute | solution.py:37
  82.0 4.9 %collective-permute-start.15 = (f32[36,256]{1,0:T(8,128)S(1)}, f32[36,256]{1,0:T(8,128)S(1)}, u32[]{:S(2)}, u32[]{:S(2)}) collective-permute-start(f32[36,256]{1,0:T(8,128)S(1)} %pad_maximum_fusion.3), channel_id=1, source_target_pairs={{0,20},{4,24},{8,28},{12,0},{16,4},{20,8},{24,12},{28,16},{1,21},{... | collective-permute-start | bytes 110600 | tf_op jit(solution)/shard_map/ppermute | solution.py:37
  83.0 4.5 %collective-permute-start.16 = (f32[36,256]{1,0:T(8,128)S(1)}, f32[36,256]{1,0:T(8,128)S(1)}, u32[]{:S(2)}, u32[]{:S(2)}) collective-permute-start(f32[36,256]{1,0:T(8,128)S(1)} %pad_maximum_fusion.3), channel_id=1, source_target_pairs={{0,24},{4,28},{8,0},{12,4},{16,8},{20,12},{24,16},{28,20},{1,25},{... | collective-permute-start | bytes 110600 | tf_op jit(solution)/shard_map/ppermute | solution.py:37
  84.6 4.2 %collective-permute-start.17 = (f32[36,256]{1,0:T(8,128)S(1)}, f32[36,256]{1,0:T(8,128)S(1)}, u32[]{:S(2)}, u32[]{:S(2)}) collective-permute-start(f32[36,256]{1,0:T(8,128)S(1)} %pad_maximum_fusion.3), channel_id=1, source_target_pairs={{0,28},{4,0},{8,4},{12,8},{16,12},{20,16},{24,20},{28,24},{1,29},{... | collective-permute-start | bytes 110600 | tf_op jit(solution)/shard_map/ppermute | solution.py:37
  93.8 2.2 %collective-permute-start.18 = (f32[8,128]{1,0:T(8,128)S(1)}, f32[8,128]{1,0:T(8,128)S(1)}, u32[]{:S(2)}, u32[]{:S(2)}) collective-permute-start(f32[8,128]{1,0:T(8,128)S(1)} %broadcast_in_dim.108), channel_id=1, source_target_pairs={{0,1},{1,0},{2,3},{3,2},{4,5},{5,4},{6,7},{7,6},{8,9},{9,8},{10,11... | collective-permute-start | bytes 12296 | tf_op jit(solution)/shard_map/ppermute | solution.py:30
  94.0 14.4 %collective-permute-start.27 = (f32[16,512]{1,0:T(8,128)S(1)}, f32[16,512]{1,0:T(8,128)S(1)}, u32[]{:S(2)}, u32[]{:S(2)}) collective-permute-start(f32[16,512]{1,0:T(8,128)S(1)} %reshape.66), channel_id=1, source_target_pairs={{0,1},{1,0},{2,3},{3,2},{4,5},{5,4},{6,7},{7,6},{8,9},{9,8},{10,11... | collective-permute-start | bytes 98312 | tf_op jit(solution)/shard_map/ppermute | solution.py:30
  94.5 16.2 %collective-permute-start.28 = (f32[16,512]{1,0:T(8,128)S(1)}, f32[16,512]{1,0:T(8,128)S(1)}, u32[]{:S(2)}, u32[]{:S(2)}) collective-permute-start(f32[16,512]{1,0:T(8,128)S(1)} %reshape.66), channel_id=1, source_target_pairs={{0,2},{1,3},{2,0},{3,1},{4,6},{5,7},{6,4},{7,5},{8,10},{9,11},{10,... | collective-permute-start | bytes 98312 | tf_op jit(solution)/shard_map/ppermute | solution.py:30
  96.7 3.7 %collective-permute-start.19 = (f32[8,128]{1,0:T(8,128)S(1)}, f32[8,128]{1,0:T(8,128)S(1)}, u32[]{:S(2)}, u32[]{:S(2)}) collective-permute-start(f32[8,128]{1,0:T(8,128)S(1)} %broadcast_add_fusion), channel_id=1, source_target_pairs={{0,2},{1,3},{2,0},{3,1},{4,6},{5,7},{6,4},{7,5},{8,10},{9,11},{10,... | collective-permute-start | bytes 12296 | tf_op jit(solution)/shard_map/ppermute | solution.py:30
  104.2 15.3 %collective-permute-start.20 = (bf16[256,256]{1,0:T(8,128)(2,1)S(1)}, bf16[256,256]{1,0:T(8,128)(2,1)S(1)}, u32[]{:S(2)}, u32[]{:S(2)}) collective-permute-start(bf16[256,256]{1,0:T(8,128)(2,1)S(1)} %get-tuple-element.10), channel_id=1, source_target_pairs={{0,4},{4,8},{8,12},{12,16},{16,20},{20,24},{24,28},{28,0},{1,5},{5... | collective-permute-start | bytes 393224 | tf_op jit(solution)/shard_map/ppermute | solution.py:37
  106.3 14.0 %collective-permute-start.21 = (bf16[256,256]{1,0:T(8,128)(2,1)S(1)}, bf16[256,256]{1,0:T(8,128)(2,1)S(1)}, u32[]{:S(2)}, u32[]{:S(2)}) collective-permute-start(bf16[256,256]{1,0:T(8,128)(2,1)S(1)} %get-tuple-element.10), channel_id=1, source_target_pairs={{0,8},{4,12},{8,16},{12,20},{16,24},{20,28},{24,0},{28,4},{1,9},{5... | collective-permute-start | bytes 393224 | tf_op jit(solution)/shard_map/ppermute | solution.py:37
  108.3 14.2 %collective-permute-start.22 = (bf16[256,256]{1,0:T(8,128)(2,1)S(1)}, bf16[256,256]{1,0:T(8,128)(2,1)S(1)}, u32[]{:S(2)}, u32[]{:S(2)}) collective-permute-start(bf16[256,256]{1,0:T(8,128)(2,1)S(1)} %get-tuple-element.10), channel_id=1, source_target_pairs={{0,12},{4,16},{8,20},{12,24},{16,28},{20,0},{24,4},{28,8},{1,13},{... | collective-permute-start | bytes 393224 | tf_op jit(solution)/shard_map/ppermute | solution.py:37
  108.4 14.9 %collective-permute-start.23 = (bf16[256,256]{1,0:T(8,128)(2,1)S(1)}, bf16[256,256]{1,0:T(8,128)(2,1)S(1)}, u32[]{:S(2)}, u32[]{:S(2)}) collective-permute-start(bf16[256,256]{1,0:T(8,128)(2,1)S(1)} %get-tuple-element.10), channel_id=1, source_target_pairs={{0,16},{4,20},{8,24},{12,28},{16,0},{20,4},{24,8},{28,12},{1,17},{... | collective-permute-start | bytes 393224 | tf_op jit(solution)/shard_map/ppermute | solution.py:37
  110.7 4.0 %collective-permute-start.29 = (f32[16,512]{1,0:T(8,128)S(1)}, f32[16,512]{1,0:T(8,128)S(1)}, u32[]{:S(2)}, u32[]{:S(2)}) collective-permute-start(f32[16,512]{1,0:T(8,128)S(1)} %collective-permute-done.27), channel_id=1, source_target_pairs={{0,2},{1,3},{2,0},{3,1},{4,6},{5,7},{6,4},{7,5},{8,10},{9,11},{10,... | collective-permute-start | bytes 98312 | tf_op jit(solution)/shard_map/ppermute | solution.py:30
  114.7 11.5 %collective-permute-start.24 = (bf16[256,256]{1,0:T(8,128)(2,1)S(1)}, bf16[256,256]{1,0:T(8,128)(2,1)S(1)}, u32[]{:S(2)}, u32[]{:S(2)}) collective-permute-start(bf16[256,256]{1,0:T(8,128)(2,1)S(1)} %get-tuple-element.10), channel_id=1, source_target_pairs={{0,20},{4,24},{8,28},{12,0},{16,4},{20,8},{24,12},{28,16},{1,21},{... | collective-permute-start | bytes 393224 | tf_op jit(solution)/shard_map/ppermute | solution.py:37
  119.5 8.4 %collective-permute-start.25 = (bf16[256,256]{1,0:T(8,128)(2,1)S(1)}, bf16[256,256]{1,0:T(8,128)(2,1)S(1)}, u32[]{:S(2)}, u32[]{:S(2)}) collective-permute-start(bf16[256,256]{1,0:T(8,128)(2,1)S(1)} %get-tuple-element.10), channel_id=1, source_target_pairs={{0,24},{4,28},{8,0},{12,4},{16,8},{20,12},{24,16},{28,20},{1,25},{... | collective-permute-start | bytes 393224 | tf_op jit(solution)/shard_map/ppermute | solution.py:37
  120.3 7.6 %collective-permute-start.26 = (bf16[256,256]{1,0:T(8,128)(2,1)S(1)}, bf16[256,256]{1,0:T(8,128)(2,1)S(1)}, u32[]{:S(2)}, u32[]{:S(2)}) collective-permute-start(bf16[256,256]{1,0:T(8,128)(2,1)S(1)} %get-tuple-element.10), channel_id=1, source_target_pairs={{0,28},{4,0},{8,4},{12,8},{16,12},{20,16},{24,20},{28,24},{1,29},{... | collective-permute-start | bytes 393224 | tf_op jit(solution)/shard_map/ppermute | solution.py:37
  128.0 1.0 copy-start.5

commit v2 on v1

v2 whole, which is shorter than its diff:
```python
import jax
import jax.numpy as jnp
from jax import lax
from jax.experimental import pallas as pl
from jax.experimental.pallas import tpu as pltpu
from jax.sharding import PartitionSpec as P

BETA_ONE = 0.9
BETA_TWO = 0.99
ADAM_EPS = 1e-08
RMS_EPS = 1e-06
LEARN_RATE = 0.05
VMEM_BYTES = 24 * 1024 * 1024
TOKEN_DIMS = (((0,), (0,)), ((), ()))
F32 = jnp.float32
BF16 = jnp.bfloat16


def adam_direction(moment_one, moment_two, gradient):
    mean_new = BETA_ONE * moment_one + (1.0 - BETA_ONE) * gradient
    second_new = BETA_TWO * moment_two + (1.0 - BETA_TWO) * gradient * gradient
    return (mean_new, second_new, mean_new / (jnp.sqrt(second_new) + ADAM_EPS))


def split_two(wide):
    high = lax.reduce_precision(wide, 8, 7)
    return high.astype(BF16), (wide - high).astype(BF16)


def swap(block, axis, bit):
    count = lax.axis_size(axis)
    return lax.ppermute(block, axis, [(i, i ^ bit) for i in range(count)])


def xor_bits(count):
    bits, bit = [], 1
    while bit < count:
        bits.append(bit)
        bit *= 2
    assert bit == count
    return bits


def xor_reduce_scatter(pieces, axis):
    left = list(range(len(pieces)))
    for bit in xor_bits(len(pieces)):
        sent = [o for o in left if o & bit]
        left = [o for o in left if not o & bit]
        for o in sent:
            pieces[o ^ bit] = pieces[o ^ bit] + swap(pieces[o], axis, bit)
    return pieces[0]


def xor_gather(block, axis):
    found = [block]
    for bit in xor_bits(lax.axis_size(axis)):
        found = found + [swap(part, axis, bit) for part in found]
    return found


def pair_gather(block, axis):
    pair = jnp.stack([block, swap(block, axis, 1)])
    return [pair] + [swap(pair, axis, o) for o in range(2, lax.axis_size(axis), 2)]


def whole(shape):
    return pl.BlockSpec(memory_space=pltpu.VMEM)


def run(kernel, indices, operands, shapes, name):
    return pl.pallas_call(
        kernel,
        in_specs=[pl.BlockSpec(memory_space=pltpu.SMEM)] + [whole(x.shape) for x in operands],
        out_specs=[whole(x.shape) for x in shapes],
        out_shape=shapes,
        compiler_params=pltpu.CompilerParams(vmem_limit_bytes=VMEM_BYTES),
        name=name,
    )(indices, *operands)


def assemble_factor(parts, others, indices):
    count = 2 * len(parts)
    half_rows, rank = parts[0].shape[1:]

    def kernel(index, *refs):
        out = refs[-1]
        for k in range(len(parts)):
            for side in range(2):
                member = index[0] ^ (2 * k + side)
                base = member * (2 * half_rows)
                mine = pl.multiple_of(base + index[1] * half_rows, half_rows)
                other = pl.multiple_of(base + (1 - index[1]) * half_rows, half_rows)
                out[pl.ds(mine, half_rows), :] = refs[k][side]
                out[pl.ds(other, half_rows), :] = refs[len(parts) + k][side]

    shape = jax.ShapeDtypeStruct((count * 2 * half_rows, rank), BF16)
    return run(kernel, indices, parts + others, [shape], "assemble")[0]


def update_kernel(parts, factor, rank_rows, indices):
    count = 2 * len(parts)
    total, columns = parts[0].shape[1:]
    rows = factor.shape[0]

    def kernel(index, *refs):
        pieces, matrix, raw, squares, decay, gathered = refs[:-5], *refs[-5:]
        for k in range(len(parts)):
            for side in range(2):
                member = index[0] ^ (2 * k + side)
                start = pl.multiple_of(member * rank_rows, rank_rows)
                gathered[pl.ds(start, rank_rows), :] = pieces[k][side, :rank_rows]
                decay[member] = pieces[k][side, rank_rows:]
        wide = gathered[...]
        high = wide.astype(BF16)
        low = (wide - high.astype(F32)).astype(BF16)
        block = rows // 4
        acc = jnp.zeros((8, columns), F32)
        for at in range(4):
            left = matrix[at * block : (at + 1) * block, :]
            value = jnp.dot(left, high, preferred_element_type=F32) + jnp.dot(
                left, low, preferred_element_type=F32
            )
            raw[at * block : (at + 1) * block, :] = value
            acc = acc + jnp.sum((value * value).reshape(block // 8, 8, columns), 0)
        squares[...] = jnp.full((8, 128), jnp.sum(acc), F32)

    return pl.pallas_call(
        kernel,
        in_specs=[pl.BlockSpec(memory_space=pltpu.SMEM)]
        + [whole(x.shape) for x in parts]
        + [whole(factor.shape)],
        out_specs=[
            whole((rows, columns)),
            whole((8, 128)),
            whole((count, total - rank_rows, columns)),
        ],
        out_shape=[
            jax.ShapeDtypeStruct((rows, columns), F32),
            jax.ShapeDtypeStruct((8, 128), F32),
            jax.ShapeDtypeStruct((count, total - rank_rows, columns), F32),
        ],
        scratch_shapes=[pltpu.VMEM((count * rank_rows, columns), F32)],
        compiler_params=pltpu.CompilerParams(vmem_limit_bytes=VMEM_BYTES),
        name="update",
    )(indices, *parts, factor)


def finish(raw, terms, masters, offsets, entries, indices):
    rows, columns = raw.shape
    shard = masters[0].shape[-2]

    def kernel(index, raw_ref, *refs):
        squares = refs[0][...]
        for ref in refs[1 : len(terms)]:
            squares = squares + ref[...]
        scale = lax.rsqrt(squares * (1.0 / entries) + RMS_EPS)[0:1, 0:1]
        step_ref, new_ref, copy_ref = refs[-3:]
        at = len(terms)
        for ref, members in zip(refs[at:-3], offsets):
            for side, offset in enumerate(members):
                start = pl.multiple_of((index[0] ^ offset) * shard, shard)
                step = raw_ref[pl.ds(start, shard), :] * scale
                new = ref[side] - LEARN_RATE * step
                copy_ref[pl.ds(start, shard), :] = new.astype(BF16)
                if offset == 0:
                    step_ref[...] = step
                    new_ref[...] = new

    shapes = [
        jax.ShapeDtypeStruct((shard, columns), F32),
        jax.ShapeDtypeStruct((shard, columns), F32),
        jax.ShapeDtypeStruct((rows, columns), BF16),
    ]
    return run(kernel, indices, [raw] + terms + masters, shapes, "finish")


def local(
    saved_input,
    value_cotangent,
    decay_cotangent,
    value_master,
    value_factor,
    value_mean,
    value_second,
    decay_master,
    decay_mean,
    decay_second,
):
    fs_count, tp_count = lax.axis_size("fs"), lax.axis_size("tp")
    tp_me, fs_me = lax.axis_index("tp"), lax.axis_index("fs")
    width_in, rank = saved_input.shape[1], value_factor.shape[1]
    columns = value_cotangent.shape[1] // tp_count
    heads = decay_cotangent.shape[1]
    shard_rows = value_factor.shape[0]
    half_rows = shard_rows // 2
    core = tp_me & 1
    indices = jnp.stack([fs_me, core]).astype(jnp.int32)

    half = lax.dynamic_slice_in_dim(value_factor, core * half_rows, half_rows, 0)
    pair = jnp.stack([half, swap(half, "fs", 1)])
    pair, saved_input = lax.optimization_barrier((pair, saved_input))
    mine = [pair] + [swap(pair, "fs", o) for o in range(2, fs_count, 2)]

    high, low = split_two(
        lax.dot_general(saved_input, value_cotangent, TOKEN_DIMS, preferred_element_type=F32)
    )
    decay_local = lax.dot_general(
        decay_cotangent, saved_input, TOKEN_DIMS, preferred_element_type=F32
    )
    decay_width = width_in // tp_count
    decay_terms = [
        lax.dynamic_slice_in_dim(
            decay_local, (tp_me ^ offset) * decay_width, decay_width, 1
        ).reshape(fs_count, -1, columns)
        for offset in range(tp_count)
    ]
    late, decay_terms, high, low = lax.optimization_barrier((mine[1:], decay_terms, high, low))
    mine = [pair] + list(late)
    factor = assemble_factor(mine, [swap(part, "tp", 1) for part in mine], indices)
    early, factor = lax.optimization_barrier((value_master[None], factor))

    pieces = []
    for offset in range(tp_count):
        member = tp_me ^ offset
        term = jnp.zeros((rank, columns), F32)
        for part in (high, low):
            block = lax.dynamic_slice_in_dim(part, member * columns, columns, 1)
            term = term + lax.dot_general(factor, block, TOKEN_DIMS, preferred_element_type=F32)
        pieces.append(
            jnp.concatenate(
                [
                    term.reshape(fs_count, rank // fs_count, columns),
                    decay_terms[offset],
                ],
                1,
            )
        )
    masters = {0: early}
    bits = xor_bits(fs_count)
    for bit in bits:
        masters[bit] = swap(early, "fs", bit)
    block_sum = xor_reduce_scatter(pieces, "tp")
    top = bits[-1]
    masters[top], block_sum = lax.optimization_barrier((masters[top], block_sum))
    for bit in reversed(bits):
        for offset in sorted(masters):
            if offset ^ bit not in masters and not offset & bit and offset & -offset > bit:
                masters[offset ^ bit] = swap(masters[offset], "fs", bit)
    owned = jnp.sum(lax.all_to_all(block_sum, "fs", 0, 0, tiled=True), 0)
    rank_rows = rank // fs_count
    projected, decay_part = owned[:rank_rows], owned[rank_rows:]
    mean_new, second_new, direction = adam_direction(value_mean, value_second, projected)

    spread = pair_gather(jnp.concatenate([direction, decay_part], 0), "fs")
    raw_all, squares, decay_block = update_kernel(spread, factor, rank_rows, indices)
    for bit in xor_bits(tp_count)[:-1]:
        squares = squares + swap(squares, "tp", bit)
    terms = [squares] + [swap(squares, "tp", bit) for bit in xor_bits(tp_count)[-1:]]
    entries = width_in * value_cotangent.shape[1]
    value_step, value_new, value_copy = finish(
        raw_all,
        terms,
        [masters[offset] for offset in sorted(masters)],
        [(offset,) for offset in sorted(masters)],
        entries,
        indices,
    )

    decay_block = decay_block.reshape(heads, decay_width)
    decay_grad = jnp.zeros((heads, width_in), F32)
    for offset, part in enumerate(xor_gather(decay_block, "tp")):
        decay_grad = lax.dynamic_update_slice_in_dim(
            decay_grad, part, (tp_me ^ offset) * decay_width, 1
        )
    unused_mean, unused_second, decay_step = adam_direction(
        decay_mean, decay_second, decay_grad.T
    )
    decay_copy = (decay_master - LEARN_RATE * decay_step).astype(BF16)
    return (value_step, value_new, value_copy, mean_new, second_new, decay_step, decay_copy)


def solution(mesh):
    in_specs = (
        P(("fs", "tp"), None),
        P(("fs", "tp"), None),
        P(("fs", "tp"), None),
        P("fs", "tp"),
        P("fs", None),
        P("fs", "tp"),
        P("fs", "tp"),
        P(),
        P(),
        P(),
    )
    out_specs = (
        P("fs", "tp"),
        P("fs", "tp"),
        P(None, "tp"),
        P("fs", "tp"),
        P("fs", "tp"),
        P(),
        P(),
    )
    return jax.shard_map(local, mesh=mesh, in_specs=in_specs, out_specs=out_specs, check_vma=False)
```

time: 131 us -> 112 us (0.85); the launches traced: 129 us -> 111 us
  waiting for transfers between devices: 22.7 us -> 36.5 us
  blocking collectives: 13.1 us -> 0 us
  other arithmetic: 14.2 us -> 3.41 us
  starting transfers between devices: 41.6 us -> 32.9 us
  Pallas kernels: 0 us -> 5.49 us
  matrix products: 21.6 us -> 19.7 us
  local copies, waits for them, and re-layouts: 13.9 us -> 12.4 us
    ppermute x21 -> x0, starting transfers between devices: 36 us -> none  [direct_gather(): lax.ppermute(block, axis, [(i, (i + step) % count) for i in range(count)])]
    ppermute x9 -> x27, starting transfers between devices: 5.66 us -> 28.1 us  [swap(): return lax.ppermute(block, axis, [(i, i ^ bit) for i in range(count)])]
    ppermute x9 -> x27, waiting for transfers between devices: 14.2 us -> 27.5 us  [swap(): return lax.ppermute(block, axis, [(i, i ^ bit) for i in range(count)])]
    all_to_all x1 -> x0, blocking collectives: 13.1 us -> none  [local(): owned = jnp.sum(lax.all_to_all(block_sum, 'fs', 0, 0, tiled=True), 0)]
    dynamic_update_slice x22 -> x0, local copies, waits for them, and re-layouts: 9.67 us -> none  [direct_gather(): out = lax.dynamic_update_index_in_dim(out, part, (me - step) % count, 0)]
    all_to_all x0 -> x1, waiting for transfers between devices: none -> 9.01 us  [local(): owned = jnp.sum(lax.all_to_all(block_sum, 'fs', 0, 0, tiled=True), 0)]
    ppermute x21 -> x0, waiting for transfers between devices: 8.45 us -> none  [direct_gather(): lax.ppermute(block, axis, [(i, (i + step) % count) for i in range(count)])]
    convert_element_type x3 -> x0, other arithmetic: 6.24 us -> none  [the longest x2 6.22 us: split_two(): low = (wide - high.astype(F32)).astype(BF16)]
  transfers between devices with their start and end apart: 30 -> 28, of which waited for: 12 -> 16; matrix products, arithmetic and copies ran while one was open for 28% -> 23% of each run, Pallas kernels for 0% -> 4%
where the time goes in v2:
time: 112 us; the launch traced here: 111 us
  waiting for transfers between devices  36.5 us (33%)
  starting transfers between devices  32.9 us (29%)
  matrix products  19.7 us (18%)
  local copies, waits for them, and re-layouts  12.4 us (11%)
  Pallas kernels  5.49 us (5%)
  other arithmetic  3.41 us (3%)
    ppermute x27, starting transfers between devices, swap(): return lax.ppermute(block, axis, [(i, i ^ bit) for i in range(count)])  28.1 us
    ppermute x27, waiting for transfers between devices, swap(): return lax.ppermute(block, axis, [(i, i ^ bit) for i in range(count)])  27.5 us
    dot_general x1, matrix products, local(): lax.dot_general(saved_input, value_cotangent, TOKEN_DIMS, preferred_eleme...  12.1 us
    all_to_all x1, waiting for transfers between devices, local(): owned = jnp.sum(lax.all_to_all(block_sum, 'fs', 0, 0, tiled=True), 0)  9.01 us
    dot_general x8, matrix products, local(): lax.dot_general(factor, block, TOKEN_DIMS, preferred_element_type=F32)  6.74 us
    reshape x4, local copies, waits for them, and re-layouts, local(): decay_terms = [lax.dynamic_slice_in_dim(decay_local, (tp_me ^ offset) * d...  5.55 us
    all_to_all x1, starting transfers between devices, local(): owned = jnp.sum(lax.all_to_all(block_sum, 'fs', 0, 0, tiled=True), 0)  4.78 us
    unnamed x40, local copies, waits for them, and re-layouts  4.24 us
  transfers between devices with their start and end apart: 28, of which 16 were waited for; matrix products, arithmetic and copies ran while one was open for 23% of the time, Pallas kernels for 4%

profile of v2, /device:TPU:0, one launch (start us, length us, event | category | flops | bytes accessed | tf_op | source)
XLA Modules:
  0.0 111.4 jit_solution(13247489946631923782)
XLA Ops:
  0.7 1.0 constant_dynamic-slice_fusion
  1.7 3.0 %collective-permute-start = (bf16[128,256]{1,0:T(8,128)(2,1)S(1)}, bf16[128,256]{1,0:T(8,128)(2,1)S(1)}, u32[]{:S(2)}, u32[]{:S(2)}) collective-permute-start(bf16[128,256]{1,0:T(8,128)(2,1)S(1)} %constant_dynamic-slice_fusion), channel_id=1, source_target_pairs={{0,4},{4,0},{8,12},{12,8},{16,20},{20,16},{24,28},{28,24},{1,5},{5... | collective-permute-start | bytes 196616 | tf_op jit(solution)/shard_map/ppermute | solution.py:32
  4.6 0.8 fusion.44
  5.5 1.4 %collective-permute-done = bf16[128,256]{1,0:T(8,128)(2,1)S(1)} collective-permute-done((bf16[128,256]{1,0:T(8,128)(2,1)S(1)}, bf16[128,256]{1,0:T(8,128)(2,1)S(1)}, u32[]{:S(2)}, u32[]{:S(2)}) %collective-permute-start) | collective-permute-done | bytes 65568 | tf_op jit(solution)/shard_map/ppermute | solution.py:32
  6.9 2.2 %collective-permute-start.1 = (bf16[2,128,256]{2,1,0:T(8,128)(2,1)S(1)}, bf16[2,128,256]{2,1,0:T(8,128)(2,1)S(1)}, u32[]{:S(2)}, u32[]{:S(2)}) collective-permute-start(bf16[2,128,256]{2,1,0:T(8,128)(2,1)S(1)} %pad_maximum_fusion.2.refs_0_), channel_id=1, source_target_pairs={{0,8},{4,12},{8,0},{12,4},{16,24},{20,28},{24,16},{28,20},{1,9},{5... | collective-permute-start | bytes 393224 | tf_op jit(solution)/shard_map/ppermute | solution.py:32
  9.1 2.6 %collective-permute-start.2 = (bf16[2,128,256]{2,1,0:T(8,128)(2,1)S(1)}, bf16[2,128,256]{2,1,0:T(8,128)(2,1)S(1)}, u32[]{:S(2)}, u32[]{:S(2)}) collective-permute-start(bf16[2,128,256]{2,1,0:T(8,128)(2,1)S(1)} %pad_maximum_fusion.2.refs_0_), channel_id=1, source_target_pairs={{0,16},{4,20},{8,24},{12,28},{16,0},{20,4},{24,8},{28,12},{1,17},{... | collective-permute-start | bytes 393224 | tf_op jit(solution)/shard_map/ppermute | solution.py:32
  11.7 12.1 %fusion = (bf16[2048,1024]{1,0:T(8,128)(2,1)}, bf16[2048,1024]{1,0:T(8,128)(2,1)}) fusion(bf16[1536,2048]{1,0:T(8,128)(2,1)} %param.10, bf16[1536,1024]{1,0:T(8,128)(2,1)S(1)} %copy-done), kind=kOutput, calls=%fused_computation.2 | convolution fusion | flops 6450839552 | bytes 17825792 | tf_op jit(solution)/shard_map/dot_general | solution.py:205
  23.8 0.9 fusion.31
  24.7 0.7 dynamic-slice_bitcast_fusion
  25.4 1.4 %reshape.41 = f32[8,4,256]{2,1,0:T(4,128)} reshape(f32[16,512]{1,0:T(8,128)} %get-tuple-element.59) | data formatting | bytes 65536 | tf_op jit(solution)/shard_map/reshape | solution.py:214
  26.8 1.4 %reshape.42 = f32[8,4,256]{2,1,0:T(4,128)} reshape(f32[16,512]{1,0:T(8,128)} %get-tuple-element.58) | data formatting | bytes 65536 | tf_op jit(solution)/shard_map/reshape | solution.py:214
  28.2 1.4 %reshape.43 = f32[8,4,256]{2,1,0:T(4,128)} reshape(f32[16,512]{1,0:T(8,128)} %get-tuple-element.57) | data formatting | bytes 65536 | tf_op jit(solution)/shard_map/reshape | solution.py:214
  29.5 1.4 %reshape.44 = f32[8,4,256]{2,1,0:T(4,128)} reshape(f32[16,512]{1,0:T(8,128)} %get-tuple-element.56) | data formatting | bytes 65536 | tf_op jit(solution)/shard_map/reshape | solution.py:214
  30.9 0.6 collective-permute-start.5
  33.3 1.2 %assemble.1.refs_4_ = bf16[2048,256]{1,0:T(8,128)(2,1)S(1)} custom-call(s32[2]{0:T(128)S(1)} %pad_add_fusion.index, bf16[2,128,256]{2,1,0:T(8,128)(2,1)S(1)} %pad_maximum_fusion.2.refs_0_, bf16[2,128,256]{2,1,0:T(8,128)(2,1)S(1)} %collective-permute-done.1.refs_1_, bf16[2,128,256]{2,1,0:T(8,128)(2,1)S(1)} %collective-permute-done.2.refs_2_, ...), custom_call_target="tpu_custom_call" | custom-call | tf_op jit(solution)/shard_map/assemble/pallas_call | solution.py:71
  34.6 2.1 %fusion.7 = f32[256,256]{1,0:T(8,128)S(1)} fusion(bf16[2048,256]{1,0:T(8,128)(2,1)S(1)} %assemble.1.refs_4_, bf16[2048,1024]{1,0:T(8,128)(2,1)} %get-tuple-element.36, s32[]{:T(128)S(6)} %select_n.41), kind=kOutput, calls=%fused_computation.13 | convolution fusion | flops 268435456 | bytes 2359300 | tf_op jit(solution)/shard_map/dot_general | solution.py:228
  36.7 1.7 %convolution_add_fusion.2 = f32[256,256]{1,0:T(8,128)S(1)} fusion(f32[256,256]{1,0:T(8,128)S(1)} %fusion.7, bf16[2048,256]{1,0:T(8,128)(2,1)S(1)} %assemble.1.refs_4_, bf16[2048,1024]{1,0:T(8,128)(2,1)} %get-tuple-element.35, s32[]{:T(128)S(6)} %select_n.41), kind=kOutput, calls=%fused_computation.5 | convolution fusion | flops 268500992 | bytes 2621444 | tf_op jit(solution)/shard_map/dot_general | solution.py:228
  41.7 1.8 %collective-permute-start.11 = (f32[8,36,256]{2,1,0:T(8,128)S(1)}, f32[8,36,256]{2,1,0:T(8,128)S(1)}, u32[]{:S(2)}, u32[]{:S(2)}) collective-permute-start(f32[8,36,256]{2,1,0:T(8,128)S(1)} %maximum_add_fusion.1), channel_id=1, source_target_pairs={{0,2},{1,3},{2,0},{3,1},{4,6},{5,7},{6,4},{7,5},{8,10},{9,11},{10,... | collective-permute-start | bytes 884744 | tf_op jit(solution)/shard_map/ppermute | solution.py:32
  44.0 1.8 %collective-permute-start.8 = (f32[1,256,256]{2,1,0:T(8,128)S(1)}, f32[1,256,256]{2,1,0:T(8,128)}, u32[]{:S(2)}, u32[]{:S(2)}) collective-permute-start(f32[1,256,256]{2,1,0:T(8,128)S(1)} %bitcast.41), channel_id=1, source_target_pairs={{0,16},{4,20},{8,24},{12,28},{16,0},{20,4},{24,8},{28,12},{1,17},{... | collective-permute-start | bytes 786440 | tf_op jit(solution)/shard_map/ppermute | solution.py:32
  46.3 5.3 %collective-permute-done.11 = f32[8,36,256]{2,1,0:T(8,128)S(1)} collective-permute-done((f32[8,36,256]{2,1,0:T(8,128)S(1)}, f32[8,36,256]{2,1,0:T(8,128)S(1)}, u32[]{:S(2)}, u32[]{:S(2)}) %collective-permute-start.11) | collective-permute-done | bytes 294944 | tf_op jit(solution)/shard_map/ppermute | solution.py:32
  51.6 0.8 fusion.13
  52.4 6.4 %collective-permute-done.8.refs_6_ = f32[1,256,256]{2,1,0:T(8,128)} collective-permute-done((f32[1,256,256]{2,1,0:T(8,128)S(1)}, f32[1,256,256]{2,1,0:T(8,128)}, u32[]{:S(2)}, u32[]{:S(2)}) %collective-permute-start.8) | collective-permute-done | bytes 262176 | tf_op jit(solution)/shard_map/ppermute | solution.py:32
  58.8 4.8 %all-to-all-start = ((f32[8,36,256]{2,1,0:T(8,128)}), f32[8,36,256]{2,1,0:T(8,128)}, u32[]{:S(2)}, u32[]{:S(2)}) async-start(f32[8,36,256]{2,1,0:T(8,128)} %fusion.13), calls=%async_computation | async-start | bytes 655360 | tf_op jit(solution)/shard_map/all_to_all | solution.py:249
  63.5 2.0 %collective-permute-start.19 = (f32[1,256,256]{2,1,0:T(8,128)S(1)}, f32[1,256,256]{2,1,0:T(8,128)}, u32[]{:S(2)}, u32[]{:S(2)}) collective-permute-start(f32[1,256,256]{2,1,0:T(8,128)S(1)} %bitcast.42), channel_id=1, source_target_pairs={{0,8},{4,12},{8,0},{12,4},{16,24},{20,28},{24,16},{28,20},{1,9},{5... | collective-permute-start | bytes 786440 | tf_op jit(solution)/shard_map/ppermute | solution.py:32
  65.6 9.0 %all-to-all-done = f32[8,36,256]{2,1,0:T(8,128)} async-done(((f32[8,36,256]{2,1,0:T(8,128)}), f32[8,36,256]{2,1,0:T(8,128)}, u32[]{:S(2)}, u32[]{:S(2)}) %all-to-all-start) | async-done | bytes 294944 | tf_op jit(solution)/shard_map/all_to_all | solution.py:249
  74.6 1.0 reduce_sum.9
  75.6 0.6 add_divide_fusion
  76.3 0.7 collective-permute-start.12
  77.0 1.4 %collective-permute-start.18 = (f32[1,256,256]{2,1,0:T(8,128)S(1)}, f32[1,256,256]{2,1,0:T(8,128)}, u32[]{:S(2)}, u32[]{:S(2)}) collective-permute-start(f32[1,256,256]{2,1,0:T(8,128)S(1)} %bitcast.43), channel_id=1, source_target_pairs={{0,4},{4,0},{8,12},{12,8},{16,20},{20,16},{24,28},{28,24},{1,5},{5... | collective-permute-start | bytes 786440 | tf_op jit(solution)/shard_map/ppermute | solution.py:32
  78.4 2.4 %collective-permute-done.12 = f32[36,256]{1,0:T(8,128)S(1)} collective-permute-done((f32[36,256]{1,0:T(8,128)S(1)}, f32[36,256]{1,0:T(8,128)S(1)}, u32[]{:S(2)}, u32[]{:S(2)}) %collective-permute-start.12) | collective-permute-done | bytes 36896 | tf_op jit(solution)/shard_map/ppermute | solution.py:32
  81.3 0.8 collective-permute-start.14
  82.1 1.9 %collective-permute-start.20 = (f32[1,256,256]{2,1,0:T(8,128)}, f32[1,256,256]{2,1,0:T(8,128)}, u32[]{:S(2)}, u32[]{:S(2)}) collective-permute-start(f32[1,256,256]{2,1,0:T(8,128)} %collective-permute-done.19.refs_4_), channel_id=1, source_target_pairs={{0,4},{4,0},{8,12},{12,8},{16,20},{20,16},{24,28},{28,24},{1,5},{5... | collective-permute-start | bytes 786440 | tf_op jit(solution)/shard_map/ppermute | solution.py:32
  84.4 1.5 %collective-permute-start.21 = (f32[1,256,256]{2,1,0:T(8,128)}, f32[1,256,256]{2,1,0:T(8,128)}, u32[]{:S(2)}, u32[]{:S(2)}) collective-permute-start(f32[1,256,256]{2,1,0:T(8,128)} %collective-permute-done.8.refs_6_), channel_id=1, source_target_pairs={{0,4},{4,0},{8,12},{12,8},{16,20},{20,16},{24,28},{28,24},{1,5},{5... | collective-permute-start | bytes 786440 | tf_op jit(solution)/shard_map/ppermute | solution.py:32
  85.9 0.8 collective-permute-start.23
  87.1 2.8 %collective-permute-start.15 = (f32[2,36,256]{2,1,0:T(8,128)S(1)}, f32[2,36,256]{2,1,0:T(8,128)S(1)}, u32[]{:S(2)}, u32[]{:S(2)}) collective-permute-start(f32[2,36,256]{2,1,0:T(8,128)S(1)} %pad_maximum_fusion.3.refs_0_), channel_id=1, source_target_pairs={{0,24},{4,28},{8,16},{12,20},{16,8},{20,12},{24,0},{28,4},{1,25},{... | collective-permute-start | bytes 221192 | tf_op jit(solution)/shard_map/ppermute | solution.py:32
  89.9 3.4 %collective-permute-done.15.refs_3_ = f32[2,36,256]{2,1,0:T(8,128)S(1)} collective-permute-done((f32[2,36,256]{2,1,0:T(8,128)S(1)}, f32[2,36,256]{2,1,0:T(8,128)S(1)}, u32[]{:S(2)}, u32[]{:S(2)}) %collective-permute-start.15) | collective-permute-done | bytes 73760 | tf_op jit(solution)/shard_map/ppermute | solution.py:32
  93.3 1.2 %copy-done.2 = bf16[2048,256]{1,0:T(8,128)(2,1)S(1)} copy-done((bf16[2048,256]{1,0:T(8,128)(2,1)S(1)}, bf16[2048,256]{1,0:T(8,128)(2,1)}, u32[]{:S(2)}) %copy-start.2) | copy-done | bytes 1048600
  94.5 1.4 %update.1 = (f32[2048,256]{1,0:T(8,128)S(1)}, f32[8,128]{1,0:T(8,128)S(1)}, f32[8,4,256]{2,1,0:T(4,128)S(1)}) custom-call(s32[2]{0:T(128)S(1)} %pad_add_fusion.index, f32[2,36,256]{2,1,0:T(8,128)S(1)} %pad_maximum_fusion.3.refs_0_, f32[2,36,256]{2,1,0:T(8,128)S(1)} %collective-permute-done.13.refs_1_, f32[2,36,256]{2,1,0:T(8,128)S(1)} %collective-permute-done.14.refs_2_, ...), custom_call_target="tpu_custom_call" | custom-call | tf_op jit(solution)/shard_map/update/pallas_call | solution.py:127
  96.0 1.3 %copy-done.3 = f32[2048,256]{1,0:T(8,128)} copy-done((f32[2048,256]{1,0:T(8,128)}, f32[2048,256]{1,0:T(8,128)S(1)}, u32[]{:S(2)}) %copy-start.3) | copy-done | bytes 2097176
  97.3 1.1 %collective-permute-done.16 = f32[8,128]{1,0:T(8,128)S(1)} collective-permute-done((f32[8,128]{1,0:T(8,128)S(1)}, f32[8,128]{1,0:T(8,128)S(1)}, u32[]{:S(2)}, u32[]{:S(2)}) %collective-permute-start.16) | collective-permute-done | bytes 4128 | tf_op jit(solution)/shard_map/ppermute | solution.py:32
  98.6 0.6 collective-permute-start.17
  99.2 1.5 %collective-permute-start.25 = (f32[16,512]{1,0:T(8,128)S(1)}, f32[16,512]{1,0:T(8,128)S(1)}, u32[]{:S(2)}, u32[]{:S(2)}) collective-permute-start(f32[16,512]{1,0:T(8,128)S(1)} %reshape.49), channel_id=1, source_target_pairs={{0,2},{1,3},{2,0},{3,1},{4,6},{5,7},{6,4},{7,5},{8,10},{9,11},{10,... | collective-permute-start | bytes 98312 | tf_op jit(solution)/shard_map/ppermute | solution.py:32
  100.9 1.4 %collective-permute-done.17.refs_1_ = f32[8,128]{1,0:T(8,128)S(1)} collective-permute-done((f32[8,128]{1,0:T(8,128)S(1)}, f32[8,128]{1,0:T(8,128)S(1)}, u32[]{:S(2)}, u32[]{:S(2)}) %collective-permute-start.17) | collective-permute-done | bytes 4128 | tf_op jit(solution)/shard_map/ppermute | solution.py:32
  102.3 1.6 %copy-done.4 = f32[2048,256]{1,0:T(8,128)S(1)} copy-done((f32[2048,256]{1,0:T(8,128)S(1)}, f32[2048,256]{1,0:T(8,128)}, u32[]{:S(2)}) %copy-start.4) | copy-done | bytes 2097176
  103.9 2.8 %finish.1 = (f32[256,256]{1,0:T(8,128)}, f32[256,256]{1,0:T(8,128)}, bf16[2048,256]{1,0:T(8,128)(2,1)}) custom-call(s32[2]{0:T(128)S(1)} %pad_add_fusion.index, f32[2048,256]{1,0:T(8,128)S(1)} %copy-done.4, f32[8,128]{1,0:T(8,128)S(1)} %add.103.refs_0_, f32[8,128]{1,0:T(8,128)S(1)} %collective-permute-done.17.refs_1_, f32[1,256,256]{2,1,0:T(8,128)S(1)} %bitcast.44, ...), custom_call_target="tpu_custom_call" | custom-call | tf_op jit(solution)/shard_map/finish/pallas_call | solution.py:71
  106.7 0.5 collective-permute-start.26
  107.3 3.4 %collective-permute-done.26 = f32[16,512]{1,0:T(8,128)S(1)} collective-permute-done((f32[16,512]{1,0:T(8,128)S(1)}, f32[16,512]{1,0:T(8,128)S(1)}, u32[]{:S(2)}, u32[]{:S(2)}) %collective-permute-start.26) | collective-permute-done | bytes 32800 | tf_op jit(solution)/shard_map/ppermute | solution.py:32
  110.7 0.8 subtract_convert_fusion
  (88 shorter events, 7.8 us)
Async XLA Ops:
  0.6 11.0 %copy-start = (bf16[1536,1024]{1,0:T(8,128)(2,1)S(1)}, bf16[1536,1024]{1,0:T(8,128)(2,1)}, u32[]{:S(2)}) copy-start(bf16[1536,1024]{1,0:T(8,128)(2,1)} %param.11) | copy-start | bytes 9437188
  1.7 5.2 %collective-permute-start = (bf16[128,256]{1,0:T(8,128)(2,1)S(1)}, bf16[128,256]{1,0:T(8,128)(2,1)S(1)}, u32[]{:S(2)}, u32[]{:S(2)}) collective-permute-start(bf16[128,256]{1,0:T(8,128)(2,1)S(1)} %constant_dynamic-slice_fusion), channel_id=1, source_target_pairs={{0,4},{4,0},{8,12},{12,8},{16,20},{20,16},{24,28},{28,24},{1,5},{5... | collective-permute-start | bytes 196616 | tf_op jit(solution)/shard_map/ppermute | solution.py:32
  6.9 16.9 %slice-start = ((s8[6291456]{0:T(1024)(128)(4,1)}), s8[4194304]{0:T(1024)(128)(4,1)S(1)}, s32[]{:S(2)}) async-start(s8[6291456]{0:T(1024)(128)(4,1)} %bitcast.45), calls=%async_computation.1 | async-start | bytes 8388608
  6.9 16.9 %slice-start.1 = ((s8[6291456]{0:T(1024)(128)(4,1)}), s8[2097152]{0:T(1024)(128)(4,1)S(1)}, s32[]{:S(2)}) async-start(s8[6291456]{0:T(1024)(128)(4,1)} %bitcast.45), calls=%async_computation.2 | async-start | bytes 4194304
  6.9 16.9 %copy-start.15 = (bf16[1536,16]{0,1:T(8,128)(2,1)S(1)}, bf16[1536,16]{0,1:T(8,128)(2,1)}, u32[]{:S(2)}) copy-start(bf16[1536,16]{0,1:T(8,128)(2,1)} %param.12) | copy-start | bytes 147460
  6.9 24.0 %collective-permute-start.1 = (bf16[2,128,256]{2,1,0:T(8,128)(2,1)S(1)}, bf16[2,128,256]{2,1,0:T(8,128)(2,1)S(1)}, u32[]{:S(2)}, u32[]{:S(2)}) collective-permute-start(bf16[2,128,256]{2,1,0:T(8,128)(2,1)S(1)} %pad_maximum_fusion.2.refs_0_), channel_id=1, source_target_pairs={{0,8},{4,12},{8,0},{12,4},{16,24},{20,28},{24,16},{28,20},{1,9},{5... | collective-permute-start | bytes 393224 | tf_op jit(solution)/shard_map/ppermute | solution.py:32
  9.1 21.9 %collective-permute-start.2 = (bf16[2,128,256]{2,1,0:T(8,128)(2,1)S(1)}, bf16[2,128,256]{2,1,0:T(8,128)(2,1)S(1)}, u32[]{:S(2)}, u32[]{:S(2)}) collective-permute-start(bf16[2,128,256]{2,1,0:T(8,128)(2,1)S(1)} %pad_maximum_fusion.2.refs_0_), channel_id=1, source_target_pairs={{0,16},{4,20},{8,24},{12,28},{16,0},{20,4},{24,8},{28,12},{1,17},{... | collective-permute-start | bytes 393224 | tf_op jit(solution)/shard_map/ppermute | solution.py:32
  11.7 19.3 %collective-permute-start.3 = (bf16[2,128,256]{2,1,0:T(8,128)(2,1)S(1)}, bf16[2,128,256]{2,1,0:T(8,128)(2,1)}, u32[]{:S(2)}, u32[]{:S(2)}) collective-permute-start(bf16[2,128,256]{2,1,0:T(8,128)(2,1)S(1)} %pad_maximum_fusion.2.refs_0_), channel_id=1, source_target_pairs={{0,24},{4,28},{8,16},{12,20},{16,8},{20,12},{24,0},{28,4},{1,25},{... | collective-permute-start | bytes 393224 | tf_op jit(solution)/shard_map/ppermute | solution.py:32
  11.7 20.4 %collective-permute-start.4 = (bf16[2,128,256]{2,1,0:T(8,128)(2,1)S(1)}, bf16[2,128,256]{2,1,0:T(8,128)(2,1)}, u32[]{:S(2)}, u32[]{:S(2)}) collective-permute-start(bf16[2,128,256]{2,1,0:T(8,128)(2,1)S(1)} %pad_maximum_fusion.2.refs_0_), channel_id=1, source_target_pairs={{0,1},{1,0},{2,3},{3,2},{4,5},{5,4},{6,7},{7,6},{8,9},{9,8},{10,11... | collective-permute-start | bytes 393224 | tf_op jit(solution)/shard_map/ppermute | solution.py:32
  30.9 1.7 %collective-permute-start.5 = (bf16[2,128,256]{2,1,0:T(8,128)(2,1)S(1)}, bf16[2,128,256]{2,1,0:T(8,128)(2,1)}, u32[]{:S(2)}, u32[]{:S(2)}) collective-permute-start(bf16[2,128,256]{2,1,0:T(8,128)(2,1)S(1)} %collective-permute-done.1.refs_1_), channel_id=1, source_target_pairs={{0,1},{1,0},{2,3},{3,2},{4,5},{5,4},{6,7},{7,6},{8,9},{9,8},{10,11... | collective-permute-start | bytes 393224 | tf_op jit(solution)/shard_map/ppermute | solution.py:32
  31.5 1.5 %collective-permute-start.6 = (bf16[2,128,256]{2,1,0:T(8,128)(2,1)S(1)}, bf16[2,128,256]{2,1,0:T(8,128)(2,1)}, u32[]{:S(2)}, u32[]{:S(2)}) collective-permute-start(bf16[2,128,256]{2,1,0:T(8,128)(2,1)S(1)} %collective-permute-done.2.refs_2_), channel_id=1, source_target_pairs={{0,1},{1,0},{2,3},{3,2},{4,5},{5,4},{6,7},{7,6},{8,9},{9,8},{10,11... | collective-permute-start | bytes 393224 | tf_op jit(solution)/shard_map/ppermute | solution.py:32
  31.6 1.8 %collective-permute-start.7 = (bf16[2,128,256]{2,1,0:T(8,128)(2,1)}, bf16[2,128,256]{2,1,0:T(8,128)(2,1)}, u32[]{:S(2)}, u32[]{:S(2)}) collective-permute-start(bf16[2,128,256]{2,1,0:T(8,128)(2,1)} %collective-permute-done.3.refs_3_), channel_id=1, source_target_pairs={{0,1},{1,0},{2,3},{3,2},{4,5},{5,4},{6,7},{7,6},{8,9},{9,8},{10,11... | collective-permute-start | bytes 393224 | tf_op jit(solution)/shard_map/ppermute | solution.py:32
  32.0 6.4 %copy-start.10 = (f32[8,4,256]{2,1,0:T(4,128)S(1)}, f32[8,4,256]{2,1,0:T(4,128)}, u32[]{:S(2)}) copy-start(f32[8,4,256]{2,1,0:T(4,128)} %reshape.42) | copy-start | bytes 98308
  32.0 6.9 %copy-start.6 = (bf16[2048,1024]{1,0:T(8,128)(2,1)S(1)}, bf16[2048,1024]{1,0:T(8,128)(2,1)}, u32[]{:S(2)}) copy-start(bf16[2048,1024]{1,0:T(8,128)(2,1)} %get-tuple-element.36) | copy-start | bytes 12582916
  34.6 11.2 %copy-start.1 = (bf16[2048,256]{1,0:T(8,128)(2,1)}, bf16[2048,256]{1,0:T(8,128)(2,1)S(1)}, u32[]{:S(2)}) copy-start(bf16[2048,256]{1,0:T(8,128)(2,1)S(1)} %assemble.1.refs_4_) | copy-start | bytes 3145732
  34.6 4.8 %copy-start.7 = (bf16[2048,1024]{1,0:T(8,128)(2,1)S(1)}, bf16[2048,1024]{1,0:T(8,128)(2,1)}, u32[]{:S(2)}) copy-start(bf16[2048,1024]{1,0:T(8,128)(2,1)} %get-tuple-element.35) | copy-start | bytes 12582916
  36.7 3.2 %copy-start.9 = (f32[8,4,256]{2,1,0:T(4,128)S(1)}, f32[8,4,256]{2,1,0:T(4,128)}, u32[]{:S(2)}) copy-start(f32[8,4,256]{2,1,0:T(4,128)} %reshape.44) | copy-start | bytes 98308
  38.5 7.8 %collective-permute-start.9 = (f32[8,36,256]{2,1,0:T(8,128)S(1)}, f32[8,36,256]{2,1,0:T(8,128)S(1)}, u32[]{:S(2)}, u32[]{:S(2)}) collective-permute-start(f32[8,36,256]{2,1,0:T(8,128)S(1)} %pad_maximum_fusion), channel_id=1, source_target_pairs={{0,1},{1,0},{2,3},{3,2},{4,5},{5,4},{6,7},{7,6},{8,9},{9,8},{10,11... | collective-permute-start | bytes 884744 | tf_op jit(solution)/shard_map/ppermute | solution.py:32
  39.4 2.3 %copy-start.14 = (f32[8,4,256]{2,1,0:T(4,128)S(1)}, f32[8,4,256]{2,1,0:T(4,128)}, u32[]{:S(2)}) copy-start(f32[8,4,256]{2,1,0:T(4,128)} %reshape.43) | copy-start | bytes 98308
  40.0 4.0 %copy-start.5 = (f32[256,256]{1,0:T(8,128)S(1)}, f32[256,256]{1,0:T(8,128)}, u32[]{:S(2)}) copy-start(f32[256,256]{1,0:T(8,128)} %param.13) | copy-start | bytes 786436
  40.0 1.7 %collective-permute-start.10 = (f32[8,36,256]{2,1,0:T(8,128)S(1)}, f32[8,36,256]{2,1,0:T(8,128)S(1)}, u32[]{:S(2)}, u32[]{:S(2)}) collective-permute-start(f32[8,36,256]{2,1,0:T(8,128)S(1)} %pad_maximum_fusion.1), channel_id=1, source_target_pairs={{0,1},{1,0},{2,3},{3,2},{4,5},{5,4},{6,7},{7,6},{8,9},{9,8},{10,11... | collective-permute-start | bytes 884744 | tf_op jit(solution)/shard_map/ppermute | solution.py:32
  40.7 10.9 %copy-start.8 = (f32[8,4,256]{2,1,0:T(4,128)S(1)}, f32[8,4,256]{2,1,0:T(4,128)}, u32[]{:S(2)}) copy-start(f32[8,4,256]{2,1,0:T(4,128)} %reshape.41) | copy-start | bytes 98308
  41.2 34.4 %copy-start.16 = (f32[32,256]{1,0:T(8,128)S(1)}, f32[32,256]{1,0:T(8,128)}, u32[]{:S(2)}) copy-start(f32[32,256]{1,0:T(8,128)} %param.16) | copy-start | bytes 98308
  41.2 34.4 %copy-start.17 = (f32[32,256]{1,0:T(8,128)S(1)}, f32[32,256]{1,0:T(8,128)}, u32[]{:S(2)}) copy-start(f32[32,256]{1,0:T(8,128)} %param.15) | copy-start | bytes 98308
  41.7 9.8 %collective-permute-start.11 = (f32[8,36,256]{2,1,0:T(8,128)S(1)}, f32[8,36,256]{2,1,0:T(8,128)S(1)}, u32[]{:S(2)}, u32[]{:S(2)}) collective-permute-start(f32[8,36,256]{2,1,0:T(8,128)S(1)} %maximum_add_fusion.1), channel_id=1, source_target_pairs={{0,2},{1,3},{2,0},{3,1},{4,6},{5,7},{6,4},{7,5},{8,10},{9,11},{10,... | collective-permute-start | bytes 884744 | tf_op jit(solution)/shard_map/ppermute | solution.py:32
  44.0 14.8 %collective-permute-start.8 = (f32[1,256,256]{2,1,0:T(8,128)S(1)}, f32[1,256,256]{2,1,0:T(8,128)}, u32[]{:S(2)}, u32[]{:S(2)}) collective-permute-start(f32[1,256,256]{2,1,0:T(8,128)S(1)} %bitcast.41), channel_id=1, source_target_pairs={{0,16},{4,20},{8,24},{12,28},{16,0},{20,4},{24,8},{28,12},{1,17},{... | collective-permute-start | bytes 786440 | tf_op jit(solution)/shard_map/ppermute | solution.py:32
  58.8 15.8 %all-to-all-start = ((f32[8,36,256]{2,1,0:T(8,128)}), f32[8,36,256]{2,1,0:T(8,128)}, u32[]{:S(2)}, u32[]{:S(2)}) async-start(f32[8,36,256]{2,1,0:T(8,128)} %fusion.13), calls=%async_computation | async-start | bytes 655360 | tf_op jit(solution)/shard_map/all_to_all | solution.py:249
  63.5 18.5 %collective-permute-start.19 = (f32[1,256,256]{2,1,0:T(8,128)S(1)}, f32[1,256,256]{2,1,0:T(8,128)}, u32[]{:S(2)}, u32[]{:S(2)}) collective-permute-start(f32[1,256,256]{2,1,0:T(8,128)S(1)} %bitcast.42), channel_id=1, source_target_pairs={{0,8},{4,12},{8,0},{12,4},{16,24},{20,28},{24,16},{28,20},{1,9},{5... | collective-permute-start | bytes 786440 | tf_op jit(solution)/shard_map/ppermute | solution.py:32
  65.6 18.9 %collective-permute-start.22 = (f32[1,256,256]{2,1,0:T(8,128)}, f32[1,256,256]{2,1,0:T(8,128)}, u32[]{:S(2)}, u32[]{:S(2)}) collective-permute-start(f32[1,256,256]{2,1,0:T(8,128)} %collective-permute-done.8.refs_6_), channel_id=1, source_target_pairs={{0,8},{4,12},{8,0},{12,4},{16,24},{20,28},{24,16},{28,20},{1,9},{5... | collective-permute-start | bytes 786440 | tf_op jit(solution)/shard_map/ppermute | solution.py:32
  76.3 4.5 %collective-permute-start.12 = (f32[36,256]{1,0:T(8,128)S(1)}, f32[36,256]{1,0:T(8,128)S(1)}, u32[]{:S(2)}, u32[]{:S(2)}) collective-permute-start(f32[36,256]{1,0:T(8,128)S(1)} %get-tuple-element.61), channel_id=1, source_target_pairs={{0,4},{4,0},{8,12},{12,8},{16,20},{20,16},{24,28},{28,24},{1,5},{5... | collective-permute-start | bytes 110600 | tf_op jit(solution)/shard_map/ppermute | solution.py:32
  77.0 21.7 %collective-permute-start.18 = (f32[1,256,256]{2,1,0:T(8,128)S(1)}, f32[1,256,256]{2,1,0:T(8,128)}, u32[]{:S(2)}, u32[]{:S(2)}) collective-permute-start(f32[1,256,256]{2,1,0:T(8,128)S(1)} %bitcast.43), channel_id=1, source_target_pairs={{0,4},{4,0},{8,12},{12,8},{16,20},{20,16},{24,28},{28,24},{1,5},{5... | collective-permute-start | bytes 786440 | tf_op jit(solution)/shard_map/ppermute | solution.py:32
  80.8 5.1 %collective-permute-start.13 = (f32[2,36,256]{2,1,0:T(8,128)S(1)}, f32[2,36,256]{2,1,0:T(8,128)S(1)}, u32[]{:S(2)}, u32[]{:S(2)}) collective-permute-start(f32[2,36,256]{2,1,0:T(8,128)S(1)} %pad_maximum_fusion.3.refs_0_), channel_id=1, source_target_pairs={{0,8},{4,12},{8,0},{12,4},{16,24},{20,28},{24,16},{28,20},{1,9},{5... | collective-permute-start | bytes 221192 | tf_op jit(solution)/shard_map/ppermute | solution.py:32
  81.3 5.8 %collective-permute-start.14 = (f32[2,36,256]{2,1,0:T(8,128)S(1)}, f32[2,36,256]{2,1,0:T(8,128)S(1)}, u32[]{:S(2)}, u32[]{:S(2)}) collective-permute-start(f32[2,36,256]{2,1,0:T(8,128)S(1)} %pad_maximum_fusion.3.refs_0_), channel_id=1, source_target_pairs={{0,16},{4,20},{8,24},{12,28},{16,0},{20,4},{24,8},{28,12},{1,17},{... | collective-permute-start | bytes 221192 | tf_op jit(solution)/shard_map/ppermute | solution.py:32
  82.1 17.2 %collective-permute-start.20 = (f32[1,256,256]{2,1,0:T(8,128)}, f32[1,256,256]{2,1,0:T(8,128)}, u32[]{:S(2)}, u32[]{:S(2)}) collective-permute-start(f32[1,256,256]{2,1,0:T(8,128)} %collective-permute-done.19.refs_4_), channel_id=1, source_target_pairs={{0,4},{4,0},{8,12},{12,8},{16,20},{20,16},{24,28},{28,24},{1,5},{5... | collective-permute-start | bytes 786440 | tf_op jit(solution)/shard_map/ppermute | solution.py:32
  84.4 16.3 %collective-permute-start.21 = (f32[1,256,256]{2,1,0:T(8,128)}, f32[1,256,256]{2,1,0:T(8,128)}, u32[]{:S(2)}, u32[]{:S(2)}) collective-permute-start(f32[1,256,256]{2,1,0:T(8,128)} %collective-permute-done.8.refs_6_), channel_id=1, source_target_pairs={{0,4},{4,0},{8,12},{12,8},{16,20},{20,16},{24,28},{28,24},{1,5},{5... | collective-permute-start | bytes 786440 | tf_op jit(solution)/shard_map/ppermute | solution.py:32
  85.9 15.0 %collective-permute-start.23 = (f32[1,256,256]{2,1,0:T(8,128)}, f32[1,256,256]{2,1,0:T(8,128)}, u32[]{:S(2)}, u32[]{:S(2)}) collective-permute-start(f32[1,256,256]{2,1,0:T(8,128)} %collective-permute-done.22.refs_8_), channel_id=1, source_target_pairs={{0,4},{4,0},{8,12},{12,8},{16,20},{20,16},{24,28},{28,24},{1,5},{5... | collective-permute-start | bytes 786440 | tf_op jit(solution)/shard_map/ppermute | solution.py:32
  87.1 6.2 %collective-permute-start.15 = (f32[2,36,256]{2,1,0:T(8,128)S(1)}, f32[2,36,256]{2,1,0:T(8,128)S(1)}, u32[]{:S(2)}, u32[]{:S(2)}) collective-permute-start(f32[2,36,256]{2,1,0:T(8,128)S(1)} %pad_maximum_fusion.3.refs_0_), channel_id=1, source_target_pairs={{0,24},{4,28},{8,16},{12,20},{16,8},{20,12},{24,0},{28,4},{1,25},{... | collective-permute-start | bytes 221192 | tf_op jit(solution)/shard_map/ppermute | solution.py:32
  93.3 1.2 %copy-start.2 = (bf16[2048,256]{1,0:T(8,128)(2,1)S(1)}, bf16[2048,256]{1,0:T(8,128)(2,1)}, u32[]{:S(2)}) copy-start(bf16[2048,256]{1,0:T(8,128)(2,1)} %copy-done.1) | copy-start | bytes 3145732
  95.9 1.3 %copy-start.3 = (f32[2048,256]{1,0:T(8,128)}, f32[2048,256]{1,0:T(8,128)S(1)}, u32[]{:S(2)}) copy-start(f32[2048,256]{1,0:T(8,128)S(1)} %get-tuple-element.42.raw_ref) | copy-start | bytes 6291460
  97.3 1.2 %collective-permute-start.16 = (f32[8,128]{1,0:T(8,128)S(1)}, f32[8,128]{1,0:T(8,128)S(1)}, u32[]{:S(2)}, u32[]{:S(2)}) collective-permute-start(f32[8,128]{1,0:T(8,128)S(1)} %get-tuple-element.43), channel_id=1, source_target_pairs={{0,1},{1,0},{2,3},{3,2},{4,5},{5,4},{6,7},{7,6},{8,9},{9,8},{10,11... | collective-permute-start | bytes 12296 | tf_op jit(solution)/shard_map/ppermute | solution.py:32
  97.3 13.3 %copy-start.11 = (f32[2048,16]{0,1:T(8,128)S(1)}, f32[2048,16]{0,1:T(8,128)}, u32[]{:S(2)}) copy-start(f32[2048,16]{0,1:T(8,128)} %param.17) | copy-start | bytes 393220
  98.5 8.3 %collective-permute-start.24 = (f32[16,512]{1,0:T(8,128)S(1)}, f32[16,512]{1,0:T(8,128)S(1)}, u32[]{:S(2)}, u32[]{:S(2)}) collective-permute-start(f32[16,512]{1,0:T(8,128)S(1)} %reshape.49), channel_id=1, source_target_pairs={{0,1},{1,0},{2,3},{3,2},{4,5},{5,4},{6,7},{7,6},{8,9},{9,8},{10,11... | collective-permute-start | bytes 98312 | tf_op jit(solution)/shard_map/ppermute | solution.py:32
  98.6 3.6 %collective-permute-start.17 = (f32[8,128]{1,0:T(8,128)S(1)}, f32[8,128]{1,0:T(8,128)S(1)}, u32[]{:S(2)}, u32[]{:S(2)}) collective-permute-start(f32[8,128]{1,0:T(8,128)S(1)} %add.103.refs_0_), channel_id=1, source_target_pairs={{0,2},{1,3},{2,0},{3,1},{4,6},{5,7},{6,4},{7,5},{8,10},{9,11},{10,... | collective-permute-start | bytes 12296 | tf_op jit(solution)/shard_map/ppermute | solution.py:32
  99.2 8.0 %collective-permute-start.25 = (f32[16,512]{1,0:T(8,128)S(1)}, f32[16,512]{1,0:T(8,128)S(1)}, u32[]{:S(2)}, u32[]{:S(2)}) collective-permute-start(f32[16,512]{1,0:T(8,128)S(1)} %reshape.49), channel_id=1, source_target_pairs={{0,2},{1,3},{2,0},{3,1},{4,6},{5,7},{6,4},{7,5},{8,10},{9,11},{10,... | collective-permute-start | bytes 98312 | tf_op jit(solution)/shard_map/ppermute | solution.py:32
  102.3 1.6 %copy-start.4 = (f32[2048,256]{1,0:T(8,128)S(1)}, f32[2048,256]{1,0:T(8,128)}, u32[]{:S(2)}) copy-start(f32[2048,256]{1,0:T(8,128)} %copy-done.3) | copy-start | bytes 6291460
  103.9 6.8 %copy-start.12 = (f32[2048,16]{0,1:T(8,128)S(1)}, f32[2048,16]{0,1:T(8,128)}, u32[]{:S(2)}) copy-start(f32[2048,16]{0,1:T(8,128)} %param.19) | copy-start | bytes 393220
  103.9 6.8 %copy-start.13 = (f32[2048,16]{0,1:T(8,128)S(1)}, f32[2048,16]{0,1:T(8,128)}, u32[]{:S(2)}) copy-start(f32[2048,16]{0,1:T(8,128)} %param.18) | copy-start | bytes 393220
  106.7 3.9 %collective-permute-start.26 = (f32[16,512]{1,0:T(8,128)S(1)}, f32[16,512]{1,0:T(8,128)S(1)}, u32[]{:S(2)}, u32[]{:S(2)}) collective-permute-start(f32[16,512]{1,0:T(8,128)S(1)} %collective-permute-done.24), channel_id=1, source_target_pairs={{0,2},{1,3},{2,0},{3,1},{4,6},{5,7},{6,4},{7,5},{8,10},{9,11},{10,... | collective-permute-start | bytes 98312 | tf_op jit(solution)/shard_map/ppermute | solution.py:32
